TPU v7x, 32 devices: a whole 2x2x4 slice. The times are simulated.
32 devices in a mesh: ep: 8 (over z, y), tp: 4 (over x, core).
Axes of the slice: x: 2, y: 2, z: 4, core: 2. Of those that a mesh axis runs over, the one named last changes fastest.
Arguments:
- tokens: bfloat16 [1024, 2048], P('ep'), may hold values from -6 to 6
- cotangent: bfloat16 [1024, 2048], P('ep'), may hold values from -2 to 2
- route_weights: float32 [1024, 2], P('ep'), may hold values from 0.25 to 2.5
- routes: int32 [1024, 2], P('ep'), may hold values from 0 to 7, all different within a row; in each aligned block of 128 rows (0 to 127, 128 to 255, ...) at most 64 rows name the same one
- gate_proj: bfloat16 [8, 2048, 512], P('ep', None, 'tp'), may hold values from -0.125 to 0.125
- up_proj: bfloat16 [8, 2048, 512], P('ep', None, 'tp'), may hold values from -0.125 to 0.125
- down_proj: bfloat16 [8, 512, 2048], P('ep', 'tp'), may hold values from -0.25 to 0.25
- shared_down: bfloat16 [2048, 512], P(None, 'tp'), may hold values from -0.25 to 0.25
- shared_hidden: bfloat16 [1024, 512], P('ep', 'tp'), may hold values from -0.29882812 to 0.29882812
Outputs:
- tokens_grad: bfloat16 [1024, 2048], P('ep', 'tp')
- weights_grad: float32 [1024, 2], P('ep')
- gate_proj_grad: bfloat16 [8, 2048, 512], P('ep', None, 'tp')
- up_proj_grad: bfloat16 [8, 2048, 512], P('ep', None, 'tp')
- down_proj_grad: bfloat16 [8, 512, 2048], P('ep', 'tp')
- hidden_grad: bfloat16 [1024, 512], P('ep', 'tp')
- shared_grad: float32 [2048, 512], P('ep', 'tp')
Inputs may be any that keep to these rules, and one draw needn't show every extreme that they name: `routes`: in each aligned block of 128 rows no expert is named more than 64 times, a bound that some block reaches; the 2 experts of a row differ.
All inputs are finite; a program needn't handle non-finite values.
Results may differ from a plain program's by a relative error of at most 0.012.
Values may be sent and summed in bfloat16 or wider, within the bound.
A program may use at most 64 MiB of HBM per device.

v0:
```python
import functools

import jax
import jax.numpy as jnp
from jax import lax
from jax.experimental import pallas as pl
from jax.experimental.pallas import tpu as pltpu
from jax.sharding import PartitionSpec as P

MESH = pl.DeviceIdType.MESH
BF = jnp.bfloat16
F32 = jnp.float32
DISP, WGT, FWD_X, FWD_C, FWD_XC, RET_C, RET_X, RET_EP, RET_G, SHARE, GSUM, PAIR = range(12)


def dot_f32(a, b, dims):
    return lax.dot_general(a, b, (dims, ((), ())), preferred_element_type=F32)


def kernel(
    n,
    cap,
    tok_ref,
    cot_ref,
    rw_ref,
    rt_ref,
    wg_ref,
    wu_ref,
    wd_ref,
    sd_ref,
    sh_ref,
    otok_ref,
    ow_ref,
    og_ref,
    ou_ref,
    od_ref,
    ohid_ref,
    osh_ref,
    perm,
    sbuf,
    abuf,
    wsend,
    wrecv,
    wgu,
    wdv,
    sdv,
    gradv,
    hw,
    dgu,
    part,
    crecv,
    keep,
    xsend,
    xrecv,
    rsend,
    ret,
    gpart,
    gcore,
    gtwo,
    gx,
    gsend,
    gret,
    ssend,
    spair,
    ssum,
    srecv,
    send_sem,
    recv_sem,
    load_sem,
    store_sem,
):
    me = lax.axis_index("ep")
    tp = lax.axis_index("tp")
    tok_rows, feat = tok_ref.shape
    top = rt_ref.shape[0]
    quarter = feat // 4
    units = wg_ref.shape[1]
    core_of = lax.rem(tp, 2)
    half_of = tp // 2
    tp_c = half_of * 2 + (1 - core_of)
    tp_x = (1 - half_of) * 2 + core_of
    tp_xc = (1 - half_of) * 2 + (1 - core_of)

    def copy(kind, at, src_ref, dst_ref, ep_to, tp_to):
        return pltpu.make_async_remote_copy(
            src_ref=src_ref,
            dst_ref=dst_ref,
            send_sem=send_sem.at[kind, at],
            recv_sem=recv_sem.at[kind, at],
            device_id=(ep_to, tp_to),
            device_id_type=MESH,
        )

    loads = [
        pltpu.make_async_copy(wg_ref, wgu.at[:, pl.ds(0, units)], load_sem.at[0]),
        pltpu.make_async_copy(wu_ref, wgu.at[:, pl.ds(units, units)], load_sem.at[1]),
        pltpu.make_async_copy(wd_ref, wdv, load_sem.at[2]),
        pltpu.make_async_copy(sd_ref, sdv, load_sem.at[3]),
    ]
    barrier = pltpu.get_barrier_semaphore()
    for d in range(1, n):
        pl.semaphore_signal(
            barrier, inc=1, device_id=(jnp.bitwise_xor(me, d), tp), device_id_type=MESH
        )
    for other in (tp_c, tp_x):
        pl.semaphore_signal(barrier, inc=1, device_id=(me, other), device_id_type=MESH)

    for load in loads:
        load.start()

    names = lax.broadcasted_iota(jnp.int32, (128, tok_rows), 0)
    named_t = jnp.zeros((128, tok_rows), F32)
    weight_t = jnp.zeros((128, tok_rows), F32)
    for k in range(top):
        hit = rt_ref[k : k + 1, :] == names
        named_t = named_t + jnp.where(hit, 1.0, 0.0)
        weight_t = weight_t + jnp.where(hit, rw_ref[k : k + 1, :].astype(BF).astype(F32), 0.0)
    before = lax.broadcasted_iota(jnp.int32, (tok_rows, tok_rows), 0) < lax.broadcasted_iota(
        jnp.int32, (tok_rows, tok_rows), 1
    )
    rank_t = dot_f32(named_t.astype(BF), jnp.where(before, 1.0, 0.0).astype(BF), ((1,), (0,)))
    slot = lax.broadcasted_iota(jnp.int32, (cap, tok_rows), 0).astype(F32)
    wsend[...] = jnp.zeros_like(wsend)
    gpart[...] = jnp.zeros_like(gpart)
    for e in range(n):
        pick = jnp.where(slot == rank_t[e : e + 1, :], named_t[e : e + 1, :], 0.0).astype(BF)
        perm[e] = pick
        wrow = jnp.broadcast_to(weight_t[e : e + 1, :], (8, tok_rows)).astype(BF)
        wsend[e, :, 0:cap] = dot_f32(wrow, pick, ((1,), (1,)))
    every = perm[...].reshape(n * cap, tok_rows)
    cols = pl.ds(pl.multiple_of(tp * quarter, quarter), quarter)
    sbuf[:, 0] = dot_f32(every, tok_ref[:, cols], ((1,), (0,))).astype(BF).reshape(n, cap, quarter)
    sbuf[:, 1] = dot_f32(every, cot_ref[:, cols], ((1,), (0,))).astype(BF).reshape(n, cap, quarter)

    pl.semaphore_wait(barrier, n + 1)

    def disp(d):
        to = jnp.bitwise_xor(me, d)
        return copy(DISP, d, sbuf.at[to], abuf.at[me, tp], to, tp)

    def disp_w(d):
        to = jnp.bitwise_xor(me, d)
        return copy(WGT, d, wsend.at[to], wrecv.at[me], to, tp)

    def disp_in(d):
        of = jnp.bitwise_xor(me, d)
        return copy(DISP, d, abuf.at[of, tp], abuf.at[of, tp], of, tp)

    def disp_w_in(d):
        of = jnp.bitwise_xor(me, d)
        return copy(WGT, d, wrecv.at[of], wrecv.at[of], of, tp)

    def fwd(kind, d, block, to):
        of = jnp.bitwise_xor(me, d)
        return copy(kind, d, abuf.at[of, block], abuf.at[of, block], me, to)

    abuf[me, tp] = sbuf[me]
    wrecv[me] = wsend[me]

    half = n // 2
    for d in [half, half + 1] + list(range(1, half)):
        disp(d).start()
    for d in range(1, n):
        disp_w(d).start()

    for load in loads:
        load.wait()
    ohid_ref[...] = dot_f32(cot_ref[...], sdv[...], ((1,), (0,))).astype(BF)
    rows_each = feat // n
    for j in range(n):
        ssend[j % 2, j // 2] = dot_f32(
            cot_ref[:, j * rows_each : (j + 1) * rows_each], sh_ref[...], ((0,), (0,))
        ).astype(BF)
    odd = lax.rem(me, 2)
    pair = copy(PAIR, 0, ssend.at[1 - odd], spair, jnp.bitwise_xor(me, 1), tp)
    pair.start()

    def share(d):
        to = jnp.bitwise_xor(me, 2 * d)
        return copy(SHARE, d, ssum.at[to // 2], srecv.at[me // 2], to, tp)

    def share_in(d):
        of = jnp.bitwise_xor(me, 2 * d)
        return copy(SHARE, d, srecv.at[of // 2], srecv.at[of // 2], of, tp)

    eye = lax.broadcasted_iota(jnp.int32, (cap, cap), 0) == lax.broadcasted_iota(
        jnp.int32, (cap, cap), 1
    )

    def to_core(d):
        of = jnp.bitwise_xor(me, d)
        return copy(RET_C, d, part.at[of, 1 - core_of], crecv.at[of], me, tp_c)

    def arrive(d):
        @pl.when(d > 0)
        def _():
            disp_in(d).wait_recv()
            disp_w_in(d).wait_recv()

        fwd(FWD_X, d, tp, tp_x).start()
        fwd(FWD_C, d, tp, tp_c).start()

        @pl.when((d >= half) & (d < n - 2))
        def _():
            disp(d).wait_send()
            disp(d + 2).start()

    def pass_core(d):
        fwd(FWD_X, d, tp_x, tp_x).wait_recv()
        fwd(FWD_XC, d, tp_x, tp_c).start()

    def compute(d):
        of = jnp.bitwise_xor(me, d)
        fwd(FWD_C, d, tp_c, tp_c).wait_recv()
        fwd(FWD_XC, d, tp_xc, tp_c).wait_recv()
        both = jnp.zeros((cap, 2 * units), F32)
        backed = jnp.zeros((cap, units), F32)
        for b in range(4):
            at = slice(b * quarter, (b + 1) * quarter)
            both = both + dot_f32(abuf[of, b, 0], wgu[at, :], ((1,), (0,)))
            backed = backed + dot_f32(abuf[of, b, 1], wdv[:, at], ((1,), (1,)))
        gate = both[:, 0:units]
        upper = both[:, units : 2 * units]
        sigma = jax.nn.sigmoid(gate)
        active = gate * sigma
        hidden = (active * upper).astype(BF).astype(F32)
        wcol = jnp.sum(jnp.where(eye, wrecv[of, 0:1, 0:cap], 0.0), axis=1, keepdims=True)
        d_hidden = wcol * backed
        hw[of] = (wcol * hidden).astype(BF)
        d_both = jnp.concatenate(
            [
                (d_hidden * upper * sigma * (1.0 + gate * (1.0 - sigma))).astype(BF),
                (d_hidden * active).astype(BF),
            ],
            axis=1,
        )
        dgu[of] = d_both
        gpart[of, :, 0:cap] = lax.dot_general(
            jnp.ones((8, units), F32),
            hidden * backed,
            (((1,), (1,)), ((), ())),
            precision=lax.Precision.HIGHEST,
            preferred_element_type=F32,
        )
        for b in range(4):
            at = slice(b * quarter, (b + 1) * quarter)
            part[of, b % 2, b // 2] = dot_f32(d_both, wgu[at, :], ((1,), (1,))).astype(BF)
        to_core(d).start()

    def gate_copy(at, src_ref, dst_ref, to):
        return copy(GSUM, at, src_ref, dst_ref, me, to)

    def to_x(d):
        of = jnp.bitwise_xor(me, d)
        return copy(RET_X, d, xsend.at[of], xrecv.at[of], me, tp_x)

    def core_sum(d):
        of = jnp.bitwise_xor(me, d)
        to_core(d).wait_recv()
        xsend[of] = (
            part[of, core_of, 1 - half_of].astype(F32) + crecv[of, 1 - half_of].astype(F32)
        ).astype(BF)
        to_x(d).start()
        keep[of] = part[of, core_of, half_of].astype(F32) + crecv[of, half_of].astype(F32)

    def back(d):
        to = jnp.bitwise_xor(me, d)
        return copy(RET_EP, d, rsend.at[to], ret.at[me], to, tp)

    def back_g(d):
        to = jnp.bitwise_xor(me, d)
        return copy(RET_G, d, gsend.at[to], gret.at[me], to, tp)

    def back_in(d):
        of = jnp.bitwise_xor(me, d)
        return copy(RET_EP, d, ret.at[of], ret.at[of], of, tp)

    def back_g_in(d):
        of = jnp.bitwise_xor(me, d)
        return copy(RET_G, d, gret.at[of], gret.at[of], of, tp)

    def return_block(d):
        of = jnp.bitwise_xor(me, d)
        to_x(d).wait_recv()
        total = (keep[of] + xrecv[of].astype(F32)).astype(BF)

        @pl.when(d == 0)
        def _():
            ret[me] = total

        @pl.when(d > 0)
        def _():
            rsend[of] = total
            back(d).start()

    lag = 4

    @pl.loop(0, n + 2)
    def _(t):
        @pl.when(t < n)
        def _():
            arrive(t)

        @pl.when((t >= 1) & (t <= n))
        def _():
            compute(t - 1)

        @pl.when(t >= 2)
        def _():
            core_sum(t - 2)

        @pl.when(t >= lag)
        def _():
            return_block(t - lag)

        @pl.when(t < n)
        def _():
            pass_core(t)

        @pl.when(t == half)
        def _():
            pair.wait_recv()
            for z in range(half):
                ssum[z] = (ssend[odd, z].astype(F32) + spair[z].astype(F32)).astype(BF)
            srecv[me // 2] = ssum[me // 2]

        @pl.when(t == n - 1)
        def _():
            for other in range(1, half):
                share(other).start()

    gate_copy(0, gpart, gcore, tp_c).start()
    gate_copy(0, gpart, gcore, tp_c).wait()
    gtwo[...] = gpart[...] + gcore[...]
    gate_copy(1, gtwo, gx, tp_x).start()

    d_all = dgu[...].reshape(n * cap, 2 * units)
    h_all = hw[...].reshape(n * cap, units)
    for b in range(4):
        at = slice(b * quarter, (b + 1) * quarter)
        grad = dot_f32(abuf[:, b, 0].reshape(n * cap, quarter), d_all, ((0,), (0,))).astype(BF)
        gradv[0, at, :] = grad[:, 0:units]
        gradv[1, at, :] = grad[:, units : 2 * units]
        wdv[:, at] = dot_f32(
            h_all, abuf[:, b, 1].reshape(n * cap, quarter), ((0,), (0,))
        ).astype(BF)

    stores = [
        pltpu.make_async_copy(gradv.at[0], og_ref, store_sem.at[0]),
        pltpu.make_async_copy(gradv.at[1], ou_ref, store_sem.at[1]),
        pltpu.make_async_copy(wdv, od_ref, store_sem.at[2]),
    ]
    for store in stores:
        store.start()

    gate_copy(1, gtwo, gx, tp_x).wait()
    gsend[...] = gtwo[...] + gx[...]
    gret[me] = gsend[me]

    @pl.loop(1, n)
    def _(d):
        back_g(d).start()

    for d in range(n + 2 - lag, n):
        return_block(jnp.int32(d))

    @pl.loop(1, n)
    def _(d):
        back_g_in(d).wait_recv()

    for d in range(1, half):
        share_in(d).wait_recv()

    sums = srecv[0].astype(F32)
    for j in range(1, half):
        sums = sums + srecv[j].astype(F32)
    osh_ref[...] = sums

    pieces = []
    for e in range(n):
        row = gret[e, :, 0:cap].astype(BF)
        pieces.append(dot_f32(row, perm[e], ((1,), (0,)))[0:1, :])
    pieces.append(jnp.zeros((128 - n, tok_rows), F32))
    values = jnp.concatenate(pieces, axis=0)
    for k in range(top):
        hit = rt_ref[k : k + 1, :] == names
        ow_ref[k : k + 1, :] = jnp.sum(jnp.where(hit, values, 0.0), axis=0, keepdims=True)

    @pl.loop(1, n)
    def _(d):
        back_in(d).wait_recv()

    otok_ref[...] = dot_f32(
        perm[...].reshape(n * cap, tok_rows), ret[...].reshape(n * cap, quarter), ((0,), (0,))
    ).astype(BF)

    for store in stores:
        store.wait()

    @pl.loop(0, n)
    def _(d):
        fwd(FWD_X, d, tp, tp_x).wait_send()
        fwd(FWD_C, d, tp, tp_c).wait_send()
        fwd(FWD_XC, d, tp_x, tp_c).wait_send()
        to_core(d).wait_send()
        to_x(d).wait_send()

    @pl.loop(1, n)
    def _(d):
        back(d).wait_send()
        back_g(d).wait_send()
        disp_w(d).wait_send()

    for d in list(range(1, half)) + [n - 2, n - 1]:
        disp(d).wait_send()
    for d in range(1, half):
        share(d).wait_send()
    pair.wait_send()


def pass_on(*refs):
    count = (len(refs) - 2) // 3
    ins, outs, held = refs[:count], refs[count : 2 * count], refs[2 * count : 3 * count]
    in_sem, out_sem = refs[-2:]
    loads = [pltpu.make_async_copy(ins[i], held[i], in_sem.at[i]) for i in range(count)]
    stores = [pltpu.make_async_copy(held[i], outs[i], out_sem.at[i]) for i in range(count)]
    for load in loads:
        load.start()
    for load, store in zip(loads, stores):
        load.wait()
        store.start()
    for store in stores:
        store.wait()


def hand_over(arrays):
    count = len(arrays)
    hbm = pl.BlockSpec(memory_space=pl.ANY)
    return pl.pallas_call(
        pass_on,
        out_shape=tuple(jax.ShapeDtypeStruct(a.shape, a.dtype) for a in arrays),
        in_specs=[hbm] * count,
        out_specs=tuple([hbm] * count),
        scratch_shapes=[pltpu.VMEM(a.shape, a.dtype) for a in arrays]
        + [pltpu.SemaphoreType.DMA((count,))] * 2,
    )(*arrays)


def fused_shards(
    tokens,
    cotangent,
    route_weights,
    routes,
    gate_proj,
    up_proj,
    down_proj,
    shared_down,
    shared_hidden,
):
    n = lax.axis_size("ep")
    tok_rows, feat = tokens.shape
    units = gate_proj.shape[2]
    hid = shared_hidden.shape[1]
    cap = 2 * tok_rows * routes.shape[1] // n
    quarter = feat // 4
    out_shape = (
        jax.ShapeDtypeStruct((tok_rows, quarter), BF),
        jax.ShapeDtypeStruct(routes.shape[::-1], F32),
        jax.ShapeDtypeStruct((feat, units), BF),
        jax.ShapeDtypeStruct((feat, units), BF),
        jax.ShapeDtypeStruct((units, feat), BF),
        jax.ShapeDtypeStruct((tok_rows, hid), BF),
        jax.ShapeDtypeStruct((feat // n, hid), F32),
    )
    tiles = pltpu.VMEM((n, 8, 128), F32)
    vmem = pl.BlockSpec(memory_space=pltpu.VMEM)
    hbm = pl.BlockSpec(memory_space=pl.ANY)
    outs = pl.pallas_call(
        functools.partial(kernel, n, cap),
        out_shape=out_shape,
        in_specs=[vmem] * 4 + [hbm] * 4 + [vmem],
        out_specs=(vmem, vmem, hbm, hbm, hbm, vmem, vmem),
        scratch_shapes=[
            pltpu.VMEM((n, cap, tok_rows), BF),
            pltpu.VMEM((n, 2, cap, quarter), BF),
            pltpu.VMEM((n, 4, 2, cap, quarter), BF),
            tiles,
            tiles,
            pltpu.VMEM((feat, 2 * units), BF),
            pltpu.VMEM((units, feat), BF),
            pltpu.VMEM((feat, hid), BF),
            pltpu.VMEM((2, feat, units), BF),
            pltpu.VMEM((n, cap, units), BF),
            pltpu.VMEM((n, cap, 2 * units), BF),
            pltpu.VMEM((n, 2, 2, cap, quarter), BF),
            pltpu.VMEM((n, 2, cap, quarter), BF),
            pltpu.VMEM((n, cap, quarter), F32),
            pltpu.VMEM((n, cap, quarter), BF),
            pltpu.VMEM((n, cap, quarter), BF),
            pltpu.VMEM((n, cap, quarter), BF),
            pltpu.VMEM((n, cap, quarter), BF),
            tiles,
            tiles,
            tiles,
            tiles,
            tiles,
            tiles,
            pltpu.VMEM((2, n // 2, feat // n, hid), BF),
            pltpu.VMEM((n // 2, feat // n, hid), BF),
            pltpu.VMEM((n // 2, feat // n, hid), BF),
            pltpu.VMEM((n // 2, feat // n, hid), BF),
            pltpu.SemaphoreType.DMA((12, n)),
            pltpu.SemaphoreType.DMA((12, n)),
            pltpu.SemaphoreType.DMA((4,)),
            pltpu.SemaphoreType.DMA((3,)),
        ],
        compiler_params=pltpu.CompilerParams(
            collective_id=0, has_side_effects=True, vmem_limit_bytes=60 * 1024 * 1024
        ),
    )(
        tokens,
        cotangent,
        route_weights.T,
        routes.T,
        gate_proj[0],
        up_proj[0],
        down_proj[0],
        shared_down,
        shared_hidden,
    )
    outs = hand_over(outs)
    return outs[0], outs[1].T, outs[2][None], outs[3][None], outs[4][None], outs[5], outs[6]


def shards(*args):
    tokens, routes, gate_proj = args[0], args[3], args[4]
    n = lax.axis_size("ep")
    tok_rows, feat = tokens.shape
    fits = (
        gate_proj.shape[0] == 1
        and lax.axis_size("tp") == 4
        and tok_rows == 128
        and n in (8, 16)
        and (2 * tok_rows * routes.shape[1]) % (16 * n) == 0
        and 2 * tok_rows * routes.shape[1] // n <= 128
        and feat % 512 == 0
        and feat // n % 128 == 0
    )
    if fits:
        return fused_shards(*args)
    return plain_shards(*args)


def plain_shards(
    tokens,
    cotangent,
    route_weights,
    routes,
    gate_proj,
    up_proj,
    down_proj,
    shared_down,
    shared_hidden,
):
    tok_rows, feat_width = tokens.shape
    top_count = routes.shape[1]
    exp_local = gate_proj.shape[0]
    ep_size = lax.axis_size("ep")
    tp_size = lax.axis_size("tp")
    exp_total = exp_local * ep_size
    capacity = 2 * tok_rows * top_count // exp_total
    quarter = feat_width // tp_size
    filled = exp_total * capacity
    flat_routes = routes.reshape(-1)
    one_hot = (flat_routes[:, None] == jnp.arange(exp_total, dtype=jnp.int32)[None, :]).astype(
        jnp.int32
    )
    rank_in = jnp.sum((jnp.cumsum(one_hot, axis=0) - one_hot) * one_hot, axis=1)
    slot_ids = flat_routes * capacity + rank_in
    route_owner = jnp.arange(flat_routes.shape[0], dtype=jnp.int32) // top_count
    owner_ids = jnp.full((filled,), tok_rows, jnp.int32).at[slot_ids].set(route_owner)
    sent_weights = (
        jnp.zeros((filled,), jnp.bfloat16)
        .at[slot_ids]
        .set(route_weights.reshape(-1).astype(jnp.bfloat16))
    )
    first_col = lax.axis_index("tp") * quarter
    own_rows = lax.dynamic_slice_in_dim(tokens, first_col, quarter, 1)
    own_grads = lax.dynamic_slice_in_dim(cotangent, first_col, quarter, 1)
    sent_rows = jnp.take(own_rows, owner_ids, axis=0, mode="fill", fill_value=0)
    sent_grads = jnp.take(own_grads, owner_ids, axis=0, mode="fill", fill_value=0)
    got_rows, got_grads, got_weights = (
        lax.all_to_all(sent_rows, "ep", split_axis=0, concat_axis=0, tiled=True),
        lax.all_to_all(sent_grads, "ep", split_axis=0, concat_axis=0, tiled=True),
        lax.all_to_all(sent_weights, "ep", split_axis=0, concat_axis=0, tiled=True),
    )
    got_rows, got_grads = (
        lax.all_gather(got_rows, "tp", axis=1, tiled=True),
        lax.all_gather(got_grads, "tp", axis=1, tiled=True),
    )
    slot_rows = got_rows.reshape(ep_size, exp_local, capacity, feat_width)
    slot_grads = got_grads.reshape(ep_size, exp_local, capacity, feat_width)
    weight_col = got_weights.reshape(ep_size, exp_local, capacity, 1).astype(jnp.float32)
    gate = jnp.einsum("secd,edf->secf", slot_rows, gate_proj, preferred_element_type=jnp.float32)
    upper = jnp.einsum("secd,edf->secf", slot_rows, up_proj, preferred_element_type=jnp.float32)
    active = jax.nn.silu(gate)
    hidden = (active * upper).astype(jnp.bfloat16)
    backed = jnp.einsum("secd,efd->secf", slot_grads, down_proj, preferred_element_type=jnp.float32)
    gate_share = jnp.sum(hidden.astype(jnp.float32) * backed, axis=3)
    d_hidden = weight_col * backed
    sigma = jax.nn.sigmoid(gate)
    d_gate = (d_hidden * upper * sigma * (1.0 + gate * (1.0 - sigma))).astype(jnp.bfloat16)
    d_up = (d_hidden * active).astype(jnp.bfloat16)
    scaled = (weight_col * slot_grads).astype(jnp.bfloat16)
    down_proj_grad = jnp.einsum(
        "secf,secd->efd", hidden, scaled, preferred_element_type=jnp.float32
    ).astype(jnp.bfloat16)
    gate_proj_grad = jnp.einsum(
        "secd,secf->edf", slot_rows, d_gate, preferred_element_type=jnp.float32
    ).astype(jnp.bfloat16)
    up_proj_grad = jnp.einsum(
        "secd,secf->edf", slot_rows, d_up, preferred_element_type=jnp.float32
    ).astype(jnp.bfloat16)
    partial_value = jnp.einsum(
        "secf,edf->secd", d_gate, gate_proj, preferred_element_type=jnp.float32
    )
    partial_value = partial_value + jnp.einsum(
        "secf,edf->secd", d_up, up_proj, preferred_element_type=jnp.float32
    )
    gate_whole = lax.psum(gate_share, "tp")
    input_cols = lax.psum_scatter(
        partial_value.astype(jnp.bfloat16), "tp", scatter_dimension=3, tiled=True
    )
    back_cols, back_gate = (
        lax.all_to_all(
            input_cols.reshape(filled, quarter), "ep", split_axis=0, concat_axis=0, tiled=True
        ),
        lax.all_to_all(
            gate_whole.astype(jnp.bfloat16).reshape(filled),
            "ep",
            split_axis=0,
            concat_axis=0,
            tiled=True,
        ),
    )
    picked = back_cols[slot_ids].reshape(tok_rows, top_count, quarter)
    tokens_grad = jnp.sum(picked.astype(jnp.float32), axis=1).astype(jnp.bfloat16)
    weights_grad = back_gate[slot_ids].astype(jnp.float32).reshape(tok_rows, top_count)
    hidden_grad = jnp.dot(cotangent, shared_down, preferred_element_type=jnp.float32).astype(
        jnp.bfloat16
    )
    shared_grad = lax.psum_scatter(
        jnp.einsum("td,th->dh", cotangent, shared_hidden, preferred_element_type=jnp.float32),
        "ep",
        scatter_dimension=0,
        tiled=True,
    )
    return (
        tokens_grad,
        weights_grad,
        gate_proj_grad,
        up_proj_grad,
        down_proj_grad,
        hidden_grad,
        shared_grad,
    )


def solution(mesh):
    in_specs = (
        P("ep", None),
        P("ep", None),
        P("ep", None),
        P("ep", None),
        P("ep", None, "tp"),
        P("ep", None, "tp"),
        P("ep", "tp", None),
        P(None, "tp"),
        P("ep", "tp"),
    )
    out_specs = (
        P("ep", "tp"),
        P("ep", None),
        P("ep", None, "tp"),
        P("ep", None, "tp"),
        P("ep", "tp", None),
        P("ep", "tp"),
        P("ep", "tp"),
    )
    return jax.shard_map(shards, mesh=mesh, in_specs=in_specs, out_specs=out_specs, check_vma=False)
```

profile of v0, /device:TPU:0, one launch (start us, length us, event | category | flops | bytes accessed | tf_op | source)
XLA Modules:
  0.0 68.4 jit_solution(9844307127971570798)
XLA Ops:
  0.6 65.4 %shard_map.144 = (bf16[128,512]{1,0:T(8,128)(2,1)}, f32[2,128]{1,0:T(2,128)}, bf16[2048,128]{1,0:T(8,128)(2,1)}, bf16[2048,128]{1,0:T(8,128)(2,1)}, bf16[128,204...) custom-call(bf16[128,2048]{1,0:T(8,128)(2,1)} %tok_ref.1, bf16[128,2048]{1,0:T(8,128)(2,1)} %cot_ref.1, ...), custom_call_target="tpu_custom_call" | custom-call | tf_op jit(solution)/shard_map/pallas_call | solution.py:478
  66.0 2.4 %shard_map.145 = (bf16[128,512]{1,0:T(8,128)(2,1)}, f32[2,128]{1,0:T(2,128)}, bf16[2048,128]{1,0:T(8,128)(2,1)}, bf16[2048,128]{1,0:T(8,128)(2,1)}, bf16[128,204...) custom-call(bf16[128,512]{1,0:T(8,128)(2,1)} %get-tuple-element.21.refs_0_, ...), custom_call_target="tpu_custom_call" | custom-call | tf_op jit(solution)/shard_map/pallas_call | solution.py:439
where the time goes:
time: 68.8 us; the launch traced here: 68.4 us
  Pallas kernels  67.8 us (99%)
    pallas_call x1, Pallas kernels, fused_shards(): pl.pallas_call(functools.partial(kernel, n, cap), out_shape=out_shape, in...  65.4 us
    pallas_call x1, Pallas kernels, hand_over(): pl.pallas_call(pass_on, out_shape=tuple((jax.ShapeDtypeStruct(a.shape, a....  2.43 us

commit v1 on v0

v1 whole, which is shorter than its diff:
```python
import functools

import jax
import jax.numpy as jnp
from jax import lax
from jax.experimental import pallas as pl
from jax.experimental.pallas import tpu as pltpu
from jax.sharding import PartitionSpec as P

MESH = pl.DeviceIdType.MESH
BF = jnp.bfloat16
F32 = jnp.float32
S_ZO, S_ZR, S_TO, S_TR, S_Y, S_YW, S_FX, S_C0, S_C = range(9)
S_RC, S_RX, S_GC, S_GX, S_RE, S_RG, S_SHARE, S_PAIR, SENDS = range(9, 18)
COUNTS = {
    "ZF": 8,
    "ZT": 4,
    "Y0": 1,
    "YF": 6,
    "YW": 4,
    "FX": 6,
    "CORE": 4,
    "RC": 5,
    "RX": 5,
    "GC": 5,
    "GX": 5,
    "RE": 1,
    "RG": 1,
    "SHARE": 1,
    "PAIR": 1,
}
FIRST = {kind: sum(list(COUNTS.values())[:i]) for i, kind in enumerate(COUNTS)}
ARRIVALS = sum(COUNTS.values())


def dot_f32(a, b, dims):
    return lax.dot_general(a, b, (dims, ((), ())), preferred_element_type=F32)


def kernel(
    n,
    cap,
    tok_ref,
    cot_ref,
    rw_ref,
    rt_ref,
    wg_ref,
    wu_ref,
    wd_ref,
    sd_ref,
    sh_ref,
    otok_ref,
    ow_ref,
    og_ref,
    ou_ref,
    od_ref,
    ohid_ref,
    osh_ref,
    xg,
    rwv,
    rtv,
    shv,
    zbuf,
    tiles,
    cperm,
    perm,
    ysend,
    wysend,
    wrecv,
    abuf,
    wgu,
    wdv,
    sdv,
    gradv,
    hw,
    dgu,
    part,
    crecv,
    keep,
    xsend,
    xrecv,
    rsend,
    ret,
    gpart,
    gcore,
    gtwo,
    gx,
    gsend,
    gret,
    ssend,
    spair,
    ssum,
    srecv,
    send_sem,
    recv_sem,
    load_sem,
    store_sem,
):
    me = lax.axis_index("ep")
    tp = lax.axis_index("tp")
    tok_rows, feat = tok_ref.shape
    top = rt_ref.shape[0]
    quarter = feat // 4
    units = wg_ref.shape[1]
    planes = n // 2
    both_rows = 2 * cap
    y = lax.rem(me, 2)
    z = me // 2
    core_of = lax.rem(tp, 2)
    half_of = tp // 2
    tp_c = half_of * 2 + (1 - core_of)
    tp_x = (1 - half_of) * 2 + core_of
    tp_xc = (1 - half_of) * 2 + (1 - core_of)
    me_y = jnp.bitwise_xor(me, 1)
    inner = (z > 0) & (z < planes - 1)
    outer = (z == 0) | (z == planes - 1)
    source = [
        z,
        jnp.where(z == 0, 1, z - 1),
        jnp.where(z == 0, 2, jnp.where(z == planes - 1, planes - 2, z + 1)),
        jnp.where(z < planes // 2, planes - 1, 0),
    ]
    source[2] = jnp.where(z == planes - 1, planes - 3, source[2])

    def copy(out, kind, at, src_ref, dst_ref, ep_to, tp_to):
        return pltpu.make_async_remote_copy(
            src_ref=src_ref,
            dst_ref=dst_ref,
            send_sem=send_sem.at[out],
            recv_sem=recv_sem.at[FIRST[kind] + at],
            device_id=(ep_to, tp_to),
            device_id_type=MESH,
        )

    def landed(kind, at, whole_ref):
        copy(0, kind, at, whole_ref, whole_ref, me_y, tp).wait_recv()

    def left(out, whole_ref):
        copy(out, "ZT", 0, whole_ref, whole_ref, me_y, tp).wait_send()

    def rows(block_y):
        return pl.ds(pl.multiple_of(block_y * cap, cap), cap)

    def columns(block):
        return pl.ds(pl.multiple_of(block * quarter, quarter), quarter)

    barrier = pltpu.get_barrier_semaphore()
    for to in ((me_y, tp), (me, tp_c), (me, tp_x)):
        pl.semaphore_signal(barrier, inc=1, device_id=to, device_id_type=MESH)

    @pl.when(z > 0)
    def _():
        pl.semaphore_signal(barrier, inc=1, device_id=(me - 2, tp), device_id_type=MESH)

    @pl.when(z < planes - 1)
    def _():
        pl.semaphore_signal(barrier, inc=1, device_id=(me + 2, tp), device_id_type=MESH)

    loads = [
        pltpu.make_async_copy(src, dst, load_sem.at[i])
        for i, (src, dst) in enumerate(
            (
                (rt_ref, rtv),
                (rw_ref, rwv),
                (tok_ref, xg.at[0]),
                (cot_ref, xg.at[1]),
                (wg_ref, wgu.at[:, pl.ds(0, units)]),
                (wu_ref, wgu.at[:, pl.ds(units, units)]),
                (wd_ref, wdv),
                (sd_ref, sdv),
                (sh_ref, shv),
            )
        )
    ]
    for load in loads:
        load.start()

    before = jnp.where(
        lax.broadcasted_iota(jnp.int32, (tok_rows, tok_rows), 0)
        < lax.broadcasted_iota(jnp.int32, (tok_rows, tok_rows), 1),
        1.0,
        0.0,
    ).astype(BF)
    slot = lax.broadcasted_iota(jnp.int32, (cap, tok_rows), 0).astype(F32)
    two = jnp.where(
        lax.broadcasted_iota(jnp.int32, (8, tok_rows), 0) == 0,
        me.astype(F32),
        me_y.astype(F32),
    )
    at_zero = y == 0

    def place(values):
        low = jnp.where(at_zero, values, 0.0)
        return jnp.concatenate([low, values - low], axis=1)

    def read_tile(i):
        s = source[i]
        named = jnp.zeros((8, tok_rows), F32)
        weight = jnp.zeros((8, tok_rows), F32)
        for k in range(top):
            hit = tiles[s, k : k + 1, :] == two
            named = named + jnp.where(hit, 1.0, 0.0)
            weight = weight + jnp.where(hit, tiles[s, top + k : top + k + 1, :], 0.0)
        rank = dot_f32(named.astype(BF), before, ((1,), (0,)))
        picks = jnp.concatenate(
            [
                jnp.where(slot == rank[j : j + 1, :], named[j : j + 1, :], 0.0).astype(BF)
                for j in range(2)
            ],
            axis=0,
        )
        cperm[i] = picks
        slotted = dot_f32(weight.astype(BF), picks, ((1,), (1,)))
        wrecv[2 * s + y] = jnp.broadcast_to(place(slotted[0:1, 0:cap]), (8, both_rows))
        wysend[i] = jnp.broadcast_to(place(slotted[1:2, cap:both_rows]), (8, both_rows))
        copy(S_YW, "YW", i, wysend.at[i], wrecv.at[2 * s + y], me_y, tp).start()

    def yw_in(i):
        at = 2 * source[i] + (1 - y)
        return copy(S_YW, "YW", i, wrecv.at[at], wrecv.at[at], me_y, tp)

    def yf(i, p, block):
        at = "Y0" if i == 0 else "YF"
        src = ysend.at[planes if block is tp_x else i, p]
        dst = abuf.at[source[i], block, p, rows(y)]
        return copy(S_Y, at, 0 if i == 0 else 2 * (i - 1) + p, src, dst, me_y, tp)

    def z_own(up, p):
        to = me + 2 if up else me - 2
        return copy(S_ZO, "ZF", 2 * z + p, xg.at[p, :, columns(tp)], zbuf.at[z, p], to, tp)

    def zt_own(up):
        to = me + 2 if up else me - 2
        return copy(S_TO, "ZT", z, tiles.at[z], tiles.at[z], to, tp)

    def z_relay(i, p):
        s = source[i]
        to = jnp.where(s < z, me + 2, me - 2)
        return copy(S_ZR, "ZF", 2 * s + p, zbuf.at[s, p], zbuf.at[s, p], to, tp)

    def zt_relay(i):
        s = source[i]
        to = jnp.where(s < z, me + 2, me - 2)
        return copy(S_TR, "ZT", s, tiles.at[s], tiles.at[s], to, tp)

    def fx(i, j, p):
        block_y = y if j == 0 else 1 - y
        at = abuf.at[source[i], tp, p, rows(block_y)]
        return copy(S_FX, "FX", 2 * (i - 1) + p, at, at, me, tp_x)

    def to_core(i, p, block):
        at = abuf.at[source[i], block, p]
        if i == 0:
            at = abuf.at[source[i], block, p, rows(1 - y)]
        return copy(S_C0 if i == 0 else S_C, "CORE", i, at, at, me, tp_c)

    def pair(q):
        return copy(S_PAIR, "PAIR", 0, ssend.at[1 - y, q], spair.at[q], me_y, tp)

    def share(d):
        to = jnp.bitwise_xor(z, d)
        return copy(S_SHARE, "SHARE", 0, ssum.at[to], srecv.at[z], 2 * to + y, tp)

    def piece(i):
        if i == 0:
            return z, rows(y), cap
        if i == 1:
            return z, rows(1 - y), cap
        return source[i - 1], pl.ds(0, both_rows), both_rows

    def rc(i):
        s, at, _ = piece(i)
        return copy(S_RC, "RC", i, part.at[s, 1 - core_of, :, at], crecv.at[s, :, at], me, tp_c)

    def rx(i):
        s, at, _ = piece(i)
        return copy(S_RX, "RX", i, xsend.at[s, at], xrecv.at[s, at], me, tp_x)

    def gc(i):
        return copy(S_GC, "GC", i, gpart.at[i], gcore.at[i], me, tp_c)

    def gxc(i):
        return copy(S_GX, "GX", i, gtwo.at[i], gx.at[i], me, tp_x)

    def back(i, j):
        s = source[i]
        block_y = y if j == 0 else 1 - y
        return copy(
            S_RE, "RE", 0, rsend.at[s, rows(block_y)], ret.at[me], 2 * s + block_y, tp
        )

    def back_g(i, j):
        to = 2 * source[i] + (y if j == 0 else 1 - y)
        return copy(S_RG, "RG", 0, gsend.at[i + 1], gret.at[me], to, tp)

    def take(i, p, gate=None):
        def run():
            landed("ZF", 2 * source[i] + p, zbuf.at[source[i], p])

            @pl.when(inner)
            def _():
                z_relay(i, p).start()

        if gate is None:
            run()
        else:
            pl.when(gate)(run)

    def spread(i, p):
        moved = dot_f32(cperm[i], zbuf[source[i], p], ((1,), (0,))).astype(BF)
        abuf[source[i], tp, p, rows(y)] = moved[0:cap]
        ysend[i, p] = moved[cap:both_rows]
        yf(i, p, tp).start()
        fx(i, 0, p).start()

    def crossed(i):
        for p in range(2):
            landed("YF", 2 * (i - 1) + p, abuf.at[source[i], tp, p, rows(1 - y)])
            fx(i, 1, p).start()
            to_core(i, p, tp).start()

    def ready(i):
        yw_in(i).wait_recv()
        if i == 0:
            landed("CORE", 0, abuf.at[z, 0:2, :, rows(1 - y)])
        else:
            landed("CORE", i, abuf.at[source[i], 0:2])

    def joined(i, p):
        landed("FX", 2 * (i - 1) + p, abuf.at[source[i], tp_x, p])
        to_core(i, p, tp_x).start()

    def compute(i):
        s, at, m = piece(i)
        both = jnp.zeros((m, 2 * units), F32)
        backed = jnp.zeros((m, units), F32)
        for b in range(4):
            cols = slice(b * quarter, (b + 1) * quarter)
            both = both + dot_f32(abuf[s, b, 0, at], wgu[cols, :], ((1,), (0,)))
            backed = backed + dot_f32(abuf[s, b, 1, at], wdv[:, cols], ((1,), (1,)))
        gate = both[:, 0:units]
        upper = both[:, units : 2 * units]
        sigma = jax.nn.sigmoid(gate)
        active = gate * sigma
        hidden = (active * upper).astype(BF).astype(F32)
        if i == 0:
            wrow, first = wrecv[me, 0:1, :], y * cap
        elif i == 1:
            wrow, first = wrecv[me_y, 0:1, :], (1 - y) * cap
        else:
            wrow, first = wrecv[2 * s, 0:1, :] + wrecv[2 * s + 1, 0:1, :], 0
        eye = (
            lax.broadcasted_iota(jnp.int32, (m, both_rows), 0) + first
            == lax.broadcasted_iota(jnp.int32, (m, both_rows), 1)
        )
        wcol = jnp.sum(jnp.where(eye, wrow, 0.0), axis=1, keepdims=True)
        d_hidden = wcol * backed
        hw[s, at] = (wcol * hidden).astype(BF)
        d_both = jnp.concatenate(
            [
                (d_hidden * upper * sigma * (1.0 + gate * (1.0 - sigma))).astype(BF),
                (d_hidden * active).astype(BF),
            ],
            axis=1,
        )
        dgu[s, at] = d_both
        for b in range(4):
            cols = slice(b * quarter, (b + 1) * quarter)
            part[s, b % 2, b // 2, at] = dot_f32(d_both, wgu[cols, :], ((1,), (1,))).astype(BF)
        rc(i).start()
        sums = lax.dot_general(
            jnp.ones((8, units), F32),
            hidden * backed,
            (((1,), (1,)), ((), ())),
            precision=lax.Precision.HIGHEST,
            preferred_element_type=F32,
        )
        if i == 0:
            sums = place(sums)
        elif i == 1:
            low = jnp.where(at_zero, 0.0, sums)
            sums = jnp.concatenate([low, sums - low], axis=1)
        gpart[i] = sums
        gc(i).start()

    def core_sum(i):
        s, at, _ = piece(i)
        rc(i).wait_recv()
        xsend[s, at] = (
            part[s, core_of, 1 - half_of, at].astype(F32) + crecv[s, 1 - half_of, at].astype(F32)
        ).astype(BF)
        rx(i).start()
        gc(i).wait_recv()
        gtwo[i] = gpart[i] + gcore[i]
        gxc(i).start()
        keep[s, at] = part[s, core_of, half_of, at].astype(F32) + crecv[s, half_of, at].astype(F32)

    def give_back(i):
        s, at, _ = piece(i)
        rx(i).wait_recv()
        total = (keep[s, at] + xrecv[s, at].astype(F32)).astype(BF)
        if i == 0:
            ret[me] = total
        else:
            rsend[s, at] = total
            if i == 1:
                back(0, 1).start()
            else:
                back(i - 1, 0).start()
                back(i - 1, 1).start()
        gxc(i).wait_recv()
        summed = gtwo[i] + gx[i]
        if i == 0:
            gret[me] = summed
        else:
            gsend[i] = summed
            if i == 1:
                back_g(0, 1).start()
            else:
                back_g(i - 1, 0).start()
                back_g(i - 1, 1).start()

    for load in loads[0:2]:
        load.wait()
    tiles[z] = jnp.concatenate(
        [
            rtv[...].astype(F32),
            rwv[...].astype(BF).astype(F32),
            jnp.zeros((8 - 2 * top, tok_rows), F32),
        ],
        axis=0,
    )
    for load in loads[2:4]:
        load.wait()
    pl.semaphore_wait(
        barrier, 3 + jnp.where(z > 0, 1, 0) + jnp.where(z < planes - 1, 1, 0)
    )

    for up, there in ((True, z < planes - 1), (False, z > 0)):

        @pl.when(there)
        def _():
            zt_own(up).start()
            z_own(up, 0).start()
            z_own(up, 1).start()

    read_tile(0)
    other = cperm[0, cap:both_rows, :]
    for p in range(2):
        ysend[0, p] = dot_f32(other, xg[p, :, columns(tp)], ((1,), (0,))).astype(BF)
        yf(0, p, tp).start()
        ysend[planes, p] = dot_f32(other, xg[p, :, columns(tp_x)], ((1,), (0,))).astype(BF)
        yf(0, p, tp_x).start()
    own = cperm[0, 0:cap, :]
    for b in range(4):
        for p in range(2):
            abuf[z, b, p, rows(y)] = dot_f32(
                own, xg[p, :, b * quarter : (b + 1) * quarter], ((1,), (0,))
            ).astype(BF)
    for load in loads[4:9]:
        load.wait()
    compute(0)

    def tile_in(i):
        landed("ZT", source[i], tiles.at[source[i]])

        @pl.when(inner)
        def _():
            zt_relay(i).start()

    tile_in(1)
    pl.when(inner)(functools.partial(tile_in, 2))
    read_tile(1)
    ohid_ref[...] = dot_f32(xg[1], sdv[...], ((1,), (0,))).astype(BF)
    rows_each = feat // n
    for j in range(n):
        ssend[j % 2, j // 2] = dot_f32(
            xg[1, :, j * rows_each : (j + 1) * rows_each], shv[...], ((0,), (0,))
        ).astype(BF)

    take(1, 0)
    take(2, 0, inner)
    spread(1, 0)
    core_sum(0)
    pair(0).start()
    take(1, 1)
    take(2, 1, inner)
    spread(1, 1)
    pair(1).start()
    landed("Y0", 0, abuf.at[z, 0:2, :, rows(1 - y)])
    for p in range(2):
        to_core(0, p, tp).start()
        to_core(0, p, tp_x).start()
    pl.when(inner)(functools.partial(tile_in, 3))
    crossed(1)
    ready(0)
    compute(1)
    pl.when(outer)(functools.partial(tile_in, 2))
    take(2, 0, outer)
    read_tile(2)
    take(3, 0, inner)
    spread(2, 0)
    pair(2).start()
    joined(1, 0)
    core_sum(1)
    take(2, 1, outer)
    take(3, 1, inner)
    spread(2, 1)
    pair(3).start()
    joined(1, 1)
    crossed(2)

    ready(1)
    compute(2)
    give_back(0)
    pl.when(outer)(functools.partial(tile_in, 3))
    take(3, 0, outer)
    read_tile(3)
    spread(3, 0)
    core_sum(2)
    joined(2, 0)
    take(3, 1, outer)
    spread(3, 1)
    joined(2, 1)
    give_back(1)
    crossed(3)
    ready(2)
    compute(3)

    names = lax.broadcasted_iota(jnp.int32, (128, tok_rows), 0)
    named_t = jnp.zeros((128, tok_rows), F32)
    for k in range(top):
        named_t = named_t + jnp.where(rtv[k : k + 1, :] == names, 1.0, 0.0)
    rank_t = dot_f32(named_t.astype(BF), before, ((1,), (0,)))
    for e in range(n):
        perm[e] = jnp.where(slot == rank_t[e : e + 1, :], named_t[e : e + 1, :], 0.0).astype(BF)

    give_back(2)
    core_sum(3)
    landed("PAIR", 0, spair)
    for q in range(planes):
        ssum[q] = (ssend[y, q].astype(F32) + spair[q].astype(F32)).astype(BF)
    srecv[z] = ssum[z]
    for d in range(1, planes):
        share(d).start()
    joined(3, 0)
    joined(3, 1)
    ready(3)
    compute(4)
    give_back(3)
    core_sum(4)

    d_all = dgu[...].reshape(n * cap, 2 * units)
    h_all = hw[...].reshape(n * cap, units)
    for b in range(4):
        at = slice(b * quarter, (b + 1) * quarter)
        grad = dot_f32(abuf[:, b, 0].reshape(n * cap, quarter), d_all, ((0,), (0,))).astype(BF)
        gradv[0, at, :] = grad[:, 0:units]
        gradv[1, at, :] = grad[:, units : 2 * units]
        wdv[:, at] = dot_f32(
            h_all, abuf[:, b, 1].reshape(n * cap, quarter), ((0,), (0,))
        ).astype(BF)

    stores = [
        pltpu.make_async_copy(gradv.at[0], og_ref, store_sem.at[0]),
        pltpu.make_async_copy(gradv.at[1], ou_ref, store_sem.at[1]),
        pltpu.make_async_copy(wdv, od_ref, store_sem.at[2]),
    ]
    for store in stores:
        store.start()

    give_back(4)

    landed("SHARE", 0, srecv.at[0 : planes - 1])
    sums = srecv[0].astype(F32)
    for j in range(1, planes):
        sums = sums + srecv[j].astype(F32)
    osh_ref[...] = sums

    landed("RG", 0, gret.at[0 : n - 1])
    pieces = []
    for e in range(n):
        full = gret[e]
        row = jnp.where(at_zero, full[:, 0:cap], full[:, cap:both_rows]).astype(BF)
        pieces.append(dot_f32(row, perm[e], ((1,), (0,)))[0:1, :])
    pieces.append(jnp.zeros((128 - n, tok_rows), F32))
    values = jnp.concatenate(pieces, axis=0)
    for k in range(top):
        hit = rtv[k : k + 1, :] == names
        ow_ref[k : k + 1, :] = jnp.sum(jnp.where(hit, values, 0.0), axis=0, keepdims=True)

    landed("RE", 0, ret.at[0 : n - 1])
    otok_ref[...] = dot_f32(
        perm[...].reshape(n * cap, tok_rows), ret[...].reshape(n * cap, quarter), ((0,), (0,))
    ).astype(BF)

    for store in stores:
        store.wait()

    @pl.when(inner)
    def _():
        left(S_ZO, zbuf.at[0:2])
        left(S_TO, tiles.at[0:2])
        left(S_ZR, zbuf.at[0 : planes - 1])
        left(S_TR, tiles.at[0 : planes - 1])

    @pl.when(outer)
    def _():
        left(S_ZO, zbuf.at[0:1])
        left(S_TO, tiles.at[0:1])

    left(S_Y, ysend)
    left(S_YW, wysend)
    left(S_FX, zbuf.at[0 : planes - 1])
    left(S_C0, abuf.at[0, 0:2, :, 0:cap])
    left(S_C, abuf.at[0 : planes - 1, 0:2])
    left(S_RC, crecv)
    left(S_RX, xsend)
    left(S_GC, gpart)
    left(S_GX, gtwo)
    left(S_RE, ret.at[0 : n - 1])
    left(S_RG, gret.at[0 : n - 1])
    left(S_SHARE, srecv.at[0 : planes - 1])
    left(S_PAIR, spair)


def pass_on(*refs):
    count = (len(refs) - 2) // 3
    ins, outs, held = refs[:count], refs[count : 2 * count], refs[2 * count : 3 * count]
    in_sem, out_sem = refs[-2:]
    loads = [pltpu.make_async_copy(ins[i], held[i], in_sem.at[i]) for i in range(count)]
    stores = [pltpu.make_async_copy(held[i], outs[i], out_sem.at[i]) for i in range(count)]
    for load in loads:
        load.start()
    for load, store in zip(loads, stores):
        load.wait()
        store.start()
    for store in stores:
        store.wait()


def hand_over(arrays):
    count = len(arrays)
    hbm = pl.BlockSpec(memory_space=pl.ANY)
    return pl.pallas_call(
        pass_on,
        out_shape=tuple(jax.ShapeDtypeStruct(a.shape, a.dtype) for a in arrays),
        in_specs=[hbm] * count,
        out_specs=tuple([hbm] * count),
        scratch_shapes=[pltpu.VMEM(a.shape, a.dtype) for a in arrays]
        + [pltpu.SemaphoreType.DMA((count,))] * 2,
    )(*arrays)


def fused_shards(
    tokens,
    cotangent,
    route_weights,
    routes,
    gate_proj,
    up_proj,
    down_proj,
    shared_down,
    shared_hidden,
):
    n = lax.axis_size("ep")
    tok_rows, feat = tokens.shape
    top = routes.shape[1]
    units = gate_proj.shape[2]
    hid = shared_hidden.shape[1]
    cap = 2 * tok_rows * top // n
    quarter = feat // 4
    planes = n // 2
    out_shape = (
        jax.ShapeDtypeStruct((tok_rows, quarter), BF),
        jax.ShapeDtypeStruct((top, tok_rows), F32),
        jax.ShapeDtypeStruct((feat, units), BF),
        jax.ShapeDtypeStruct((feat, units), BF),
        jax.ShapeDtypeStruct((units, feat), BF),
        jax.ShapeDtypeStruct((tok_rows, hid), BF),
        jax.ShapeDtypeStruct((feat // n, hid), F32),
    )
    vmem = pl.BlockSpec(memory_space=pltpu.VMEM)
    hbm = pl.BlockSpec(memory_space=pl.ANY)
    per_piece = pltpu.VMEM((planes + 1, 8, 128), F32)
    outs = pl.pallas_call(
        functools.partial(kernel, n, cap),
        out_shape=out_shape,
        in_specs=[hbm] * 9,
        out_specs=(vmem, vmem, hbm, hbm, hbm, vmem, vmem),
        scratch_shapes=[
            pltpu.VMEM((2, tok_rows, feat), BF),
            pltpu.VMEM((top, tok_rows), F32),
            pltpu.VMEM((top, tok_rows), jnp.int32),
            pltpu.VMEM((tok_rows, hid), BF),
            pltpu.VMEM((planes, 2, tok_rows, quarter), BF),
            pltpu.VMEM((planes, 8, tok_rows), F32),
            pltpu.VMEM((planes, 2 * cap, tok_rows), BF),
            pltpu.VMEM((n, cap, tok_rows), BF),
            pltpu.VMEM((planes + 1, 2, cap, quarter), BF),
            pltpu.VMEM((planes, 8, 2 * cap), F32),
            pltpu.VMEM((n, 8, 2 * cap), F32),
            pltpu.VMEM((planes, 4, 2, 2 * cap, quarter), BF),
            pltpu.VMEM((feat, 2 * units), BF),
            pltpu.VMEM((units, feat), BF),
            pltpu.VMEM((feat, hid), BF),
            pltpu.VMEM((2, feat, units), BF),
            pltpu.VMEM((planes, 2 * cap, units), BF),
            pltpu.VMEM((planes, 2 * cap, 2 * units), BF),
            pltpu.VMEM((planes, 2, 2, 2 * cap, quarter), BF),
            pltpu.VMEM((planes, 2, 2 * cap, quarter), BF),
            pltpu.VMEM((planes, 2 * cap, quarter), F32),
            pltpu.VMEM((planes, 2 * cap, quarter), BF),
            pltpu.VMEM((planes, 2 * cap, quarter), BF),
            pltpu.VMEM((planes, 2 * cap, quarter), BF),
            pltpu.VMEM((n, cap, quarter), BF),
            per_piece,
            per_piece,
            per_piece,
            per_piece,
            per_piece,
            pltpu.VMEM((n, 8, 128), F32),
            pltpu.VMEM((2, planes, feat // n, hid), BF),
            pltpu.VMEM((planes, feat // n, hid), BF),
            pltpu.VMEM((planes, feat // n, hid), BF),
            pltpu.VMEM((planes, feat // n, hid), BF),
            pltpu.SemaphoreType.DMA((SENDS,)),
            pltpu.SemaphoreType.DMA((ARRIVALS,)),
            pltpu.SemaphoreType.DMA((9,)),
            pltpu.SemaphoreType.DMA((3,)),
        ],
        compiler_params=pltpu.CompilerParams(
            collective_id=0, has_side_effects=True, vmem_limit_bytes=60 * 1024 * 1024
        ),
    )(
        tokens,
        cotangent,
        route_weights.T,
        routes.T,
        gate_proj[0],
        up_proj[0],
        down_proj[0],
        shared_down,
        shared_hidden,
    )
    outs = hand_over(outs)
    return outs[0], outs[1].T, outs[2][None], outs[3][None], outs[4][None], outs[5], outs[6]


def shards(*args):
    tokens, routes, gate_proj = args[0], args[3], args[4]
    n = lax.axis_size("ep")
    tok_rows, feat = tokens.shape
    top = routes.shape[1]
    fits = (
        gate_proj.shape[0] == 1
        and lax.axis_size("tp") == 4
        and n == 8
        and tok_rows == 128
        and 4 * tok_rows * top == n * tok_rows
        and 2 * top <= 8
        and feat % 512 == 0
        and feat // n % 128 == 0
    )
    if fits:
        return fused_shards(*args)
    return plain_shards(*args)


def plain_shards(
    tokens,
    cotangent,
    route_weights,
    routes,
    gate_proj,
    up_proj,
    down_proj,
    shared_down,
    shared_hidden,
):
    tok_rows, feat_width = tokens.shape
    top_count = routes.shape[1]
    exp_local = gate_proj.shape[0]
    ep_size = lax.axis_size("ep")
    tp_size = lax.axis_size("tp")
    exp_total = exp_local * ep_size
    capacity = 2 * tok_rows * top_count // exp_total
    quarter = feat_width // tp_size
    filled = exp_total * capacity
    flat_routes = routes.reshape(-1)
    one_hot = (flat_routes[:, None] == jnp.arange(exp_total, dtype=jnp.int32)[None, :]).astype(
        jnp.int32
    )
    rank_in = jnp.sum((jnp.cumsum(one_hot, axis=0) - one_hot) * one_hot, axis=1)
    slot_ids = flat_routes * capacity + rank_in
    route_owner = jnp.arange(flat_routes.shape[0], dtype=jnp.int32) // top_count
    owner_ids = jnp.full((filled,), tok_rows, jnp.int32).at[slot_ids].set(route_owner)
    sent_weights = (
        jnp.zeros((filled,), jnp.bfloat16)
        .at[slot_ids]
        .set(route_weights.reshape(-1).astype(jnp.bfloat16))
    )
    first_col = lax.axis_index("tp") * quarter
    own_rows = lax.dynamic_slice_in_dim(tokens, first_col, quarter, 1)
    own_grads = lax.dynamic_slice_in_dim(cotangent, first_col, quarter, 1)
    sent_rows = jnp.take(own_rows, owner_ids, axis=0, mode="fill", fill_value=0)
    sent_grads = jnp.take(own_grads, owner_ids, axis=0, mode="fill", fill_value=0)
    got_rows, got_grads, got_weights = (
        lax.all_to_all(sent_rows, "ep", split_axis=0, concat_axis=0, tiled=True),
        lax.all_to_all(sent_grads, "ep", split_axis=0, concat_axis=0, tiled=True),
        lax.all_to_all(sent_weights, "ep", split_axis=0, concat_axis=0, tiled=True),
    )
    got_rows, got_grads = (
        lax.all_gather(got_rows, "tp", axis=1, tiled=True),
        lax.all_gather(got_grads, "tp", axis=1, tiled=True),
    )
    slot_rows = got_rows.reshape(ep_size, exp_local, capacity, feat_width)
    slot_grads = got_grads.reshape(ep_size, exp_local, capacity, feat_width)
    weight_col = got_weights.reshape(ep_size, exp_local, capacity, 1).astype(jnp.float32)
    gate = jnp.einsum("secd,edf->secf", slot_rows, gate_proj, preferred_element_type=jnp.float32)
    upper = jnp.einsum("secd,edf->secf", slot_rows, up_proj, preferred_element_type=jnp.float32)
    active = jax.nn.silu(gate)
    hidden = (active * upper).astype(jnp.bfloat16)
    backed = jnp.einsum("secd,efd->secf", slot_grads, down_proj, preferred_element_type=jnp.float32)
    gate_share = jnp.sum(hidden.astype(jnp.float32) * backed, axis=3)
    d_hidden = weight_col * backed
    sigma = jax.nn.sigmoid(gate)
    d_gate = (d_hidden * upper * sigma * (1.0 + gate * (1.0 - sigma))).astype(jnp.bfloat16)
    d_up = (d_hidden * active).astype(jnp.bfloat16)
    scaled = (weight_col * slot_grads).astype(jnp.bfloat16)
    down_proj_grad = jnp.einsum(
        "secf,secd->efd", hidden, scaled, preferred_element_type=jnp.float32
    ).astype(jnp.bfloat16)
    gate_proj_grad = jnp.einsum(
        "secd,secf->edf", slot_rows, d_gate, preferred_element_type=jnp.float32
    ).astype(jnp.bfloat16)
    up_proj_grad = jnp.einsum(
        "secd,secf->edf", slot_rows, d_up, preferred_element_type=jnp.float32
    ).astype(jnp.bfloat16)
    partial_value = jnp.einsum(
        "secf,edf->secd", d_gate, gate_proj, preferred_element_type=jnp.float32
    )
    partial_value = partial_value + jnp.einsum(
        "secf,edf->secd", d_up, up_proj, preferred_element_type=jnp.float32
    )
    gate_whole = lax.psum(gate_share, "tp")
    input_cols = lax.psum_scatter(
        partial_value.astype(jnp.bfloat16), "tp", scatter_dimension=3, tiled=True
    )
    back_cols, back_gate = (
        lax.all_to_all(
            input_cols.reshape(filled, quarter), "ep", split_axis=0, concat_axis=0, tiled=True
        ),
        lax.all_to_all(
            gate_whole.astype(jnp.bfloat16).reshape(filled),
            "ep",
            split_axis=0,
            concat_axis=0,
            tiled=True,
        ),
    )
    picked = back_cols[slot_ids].reshape(tok_rows, top_count, quarter)
    tokens_grad = jnp.sum(picked.astype(jnp.float32), axis=1).astype(jnp.bfloat16)
    weights_grad = back_gate[slot_ids].astype(jnp.float32).reshape(tok_rows, top_count)
    hidden_grad = jnp.dot(cotangent, shared_down, preferred_element_type=jnp.float32).astype(
        jnp.bfloat16
    )
    shared_grad = lax.psum_scatter(
        jnp.einsum("td,th->dh", cotangent, shared_hidden, preferred_element_type=jnp.float32),
        "ep",
        scatter_dimension=0,
        tiled=True,
    )
    return (
        tokens_grad,
        weights_grad,
        gate_proj_grad,
        up_proj_grad,
        down_proj_grad,
        hidden_grad,
        shared_grad,
    )


def solution(mesh):
    in_specs = (
        P("ep", None),
        P("ep", None),
        P("ep", None),
        P("ep", None),
        P("ep", None, "tp"),
        P("ep", None, "tp"),
        P("ep", "tp", None),
        P(None, "tp"),
        P("ep", "tp"),
    )
    out_specs = (
        P("ep", "tp"),
        P("ep", None),
        P("ep", None, "tp"),
        P("ep", None, "tp"),
        P("ep", "tp", None),
        P("ep", "tp"),
        P("ep", "tp"),
    )
    return jax.shard_map(shards, mesh=mesh, in_specs=in_specs, out_specs=out_specs, check_vma=False)
```

time: 68.8 us -> 58.5 us (0.85)
  Pallas kernels: 67.8 us -> 57.7 us
    pallas_call x1, Pallas kernels: 65.4 us -> 55.3 us  [fused_shards(): pl.pallas_call(functools.partial(kernel, n, cap), out_shape=out_shape, in...]
where the time goes in v1:
time: 58.5 us; the launch traced here: 58.4 us
  Pallas kernels  57.7 us (99%)
  between operations  0.64 us (1%)
    pallas_call x1, Pallas kernels, fused_shards(): pl.pallas_call(functools.partial(kernel, n, cap), out_shape=out_shape, in...  55.3 us
    pallas_call x1, Pallas kernels, hand_over(): pl.pallas_call(pass_on, out_shape=tuple((jax.ShapeDtypeStruct(a.shape, a....  2.43 us

profile of v1, /device:TPU:0, one launch (start us, length us, event | category | flops | bytes accessed | tf_op | source)
XLA Modules:
  0.0 58.4 jit_solution(2504210960615299991)
XLA Ops:
  0.6 55.3 %shard_map.144 = (bf16[128,512]{1,0:T(8,128)(2,1)}, f32[2,128]{1,0:T(2,128)}, bf16[2048,128]{1,0:T(8,128)(2,1)}, bf16[2048,128]{1,0:T(8,128)(2,1)}, bf16[128,204...) custom-call(bf16[128,2048]{1,0:T(8,128)(2,1)} %tok_ref.1, bf16[128,2048]{1,0:T(8,128)(2,1)} %cot_ref.1, ...), custom_call_target="tpu_custom_call" | custom-call | tf_op jit(solution)/shard_map/pallas_call | solution.py:686
  55.9 2.4 %shard_map.145 = (bf16[128,512]{1,0:T(8,128)(2,1)}, f32[2,128]{1,0:T(2,128)}, bf16[2048,128]{1,0:T(8,128)(2,1)}, bf16[2048,128]{1,0:T(8,128)(2,1)}, bf16[128,204...) custom-call(bf16[128,512]{1,0:T(8,128)(2,1)} %get-tuple-element.21.refs_0_, ...), custom_call_target="tpu_custom_call" | custom-call | tf_op jit(solution)/shard_map/pallas_call | solution.py:645

commit v2 on v1

--- a/solution.py
+++ b/solution.py
@@ -13,15 +13,15 @@
 S_ZO, S_ZR, S_TO, S_TR, S_Y, S_YW, S_FX, S_C0, S_C = range(9)
 S_RC, S_RX, S_GC, S_GX, S_RE, S_RG, S_SHARE, S_PAIR, SENDS = range(9, 18)
 COUNTS = {
-    "ZF": 8,
+    "ZF": 16,
     "ZT": 4,
     "Y0": 1,
-    "YF": 6,
+    "YF": 12,
     "YW": 4,
-    "FX": 6,
+    "FX": 12,
     "CORE": 4,
     "RC": 5,
-    "RX": 5,
+    "RX": 6,
     "GC": 5,
     "GX": 5,
     "RE": 1,
@@ -71,7 +71,6 @@
     wgu,
     wdv,
     sdv,
-    gradv,
     hw,
     dgu,
     part,
@@ -94,7 +93,6 @@
     send_sem,
     recv_sem,
     load_sem,
-    store_sem,
 ):
     me = lax.axis_index("ep")
     tp = lax.axis_index("tp")
@@ -114,13 +112,13 @@
     me_y = jnp.bitwise_xor(me, 1)
     inner = (z > 0) & (z < planes - 1)
     outer = (z == 0) | (z == planes - 1)
-    source = [
-        z,
-        jnp.where(z == 0, 1, z - 1),
-        jnp.where(z == 0, 2, jnp.where(z == planes - 1, planes - 2, z + 1)),
-        jnp.where(z < planes // 2, planes - 1, 0),
-    ]
-    source[2] = jnp.where(z == planes - 1, planes - 3, source[2])
+    low_inner = z == 1
+    high_inner = z == planes - 2
+    first = jnp.where(z == 0, 1, z - 1)
+    second = jnp.where(z == 0, 2, jnp.where(low_inner, z + 1, 0))
+    source = [z, first, second, jnp.where(z == planes - 1, 1, planes - 1)]
+    pieces_of = range(4)
+    part_cols = quarter // 2
 
     def copy(out, kind, at, src_ref, dst_ref, ep_to, tp_to):
         return pltpu.make_async_remote_copy(
@@ -140,6 +138,9 @@
 
     def rows(block_y):
         return pl.ds(pl.multiple_of(block_y * cap, cap), cap)
+
+    def split(c):
+        return c // 2, pl.ds((c % 2) * part_cols, part_cols)
 
     def columns(block):
         return pl.ds(pl.multiple_of(block * quarter, quarter), quarter)
@@ -219,43 +220,61 @@
         at = 2 * source[i] + (1 - y)
         return copy(S_YW, "YW", i, wrecv.at[at], wrecv.at[at], me_y, tp)
 
-    def yf(i, p, block):
-        at = "Y0" if i == 0 else "YF"
-        src = ysend.at[planes if block is tp_x else i, p]
-        dst = abuf.at[source[i], block, p, rows(y)]
-        return copy(S_Y, at, 0 if i == 0 else 2 * (i - 1) + p, src, dst, me_y, tp)
-
-    def z_own(up, p):
+    def yf(i, c):
+        p, at = split(c)
+        dst = abuf.at[source[i], tp, p, rows(y), at]
+        return copy(S_Y, "YF", 4 * (i - 1) + c, ysend.at[i, p, :, at], dst, me_y, tp)
+
+    def y_own(c, block):
+        p, at = split(c)
+        src = ysend.at[planes if block is tp_x else 0, p, :, at]
+        return copy(S_Y, "Y0", 0, src, abuf.at[z, block, p, rows(y), at], me_y, tp)
+
+
+    def z_own(up, c):
         to = me + 2 if up else me - 2
-        return copy(S_ZO, "ZF", 2 * z + p, xg.at[p, :, columns(tp)], zbuf.at[z, p], to, tp)
+        p, at = split(c)
+        first = pl.multiple_of(tp * quarter + (c % 2) * part_cols, part_cols)
+        src = xg.at[p, :, pl.ds(first, part_cols)]
+        return copy(S_ZO, "ZF", 4 * z + c, src, zbuf.at[z, p, :, at], to, tp)
 
     def zt_own(up):
         to = me + 2 if up else me - 2
         return copy(S_TO, "ZT", z, tiles.at[z], tiles.at[z], to, tp)
 
-    def z_relay(i, p):
+    def z_relay(i, c):
         s = source[i]
         to = jnp.where(s < z, me + 2, me - 2)
-        return copy(S_ZR, "ZF", 2 * s + p, zbuf.at[s, p], zbuf.at[s, p], to, tp)
+        p, at = split(c)
+        block = zbuf.at[s, p, :, at]
+        return copy(S_ZR, "ZF", 4 * s + c, block, block, to, tp)
 
     def zt_relay(i):
         s = source[i]
         to = jnp.where(s < z, me + 2, me - 2)
         return copy(S_TR, "ZT", s, tiles.at[s], tiles.at[s], to, tp)
 
-    def fx(i, j, p):
+    def fx(i, j, c):
         block_y = y if j == 0 else 1 - y
-        at = abuf.at[source[i], tp, p, rows(block_y)]
-        return copy(S_FX, "FX", 2 * (i - 1) + p, at, at, me, tp_x)
-
-    def to_core(i, p, block):
-        at = abuf.at[source[i], block, p]
-        if i == 0:
-            at = abuf.at[source[i], block, p, rows(1 - y)]
-        return copy(S_C0 if i == 0 else S_C, "CORE", i, at, at, me, tp_c)
+        p, at = split(c)
+        block = abuf.at[source[i], tp, p, rows(block_y), at]
+        return copy(S_FX, "FX", 4 * (i - 1) + c, block, block, me, tp_x)
+
+    def own_to_core(p, block):
+        at = abuf.at[z, block, p, rows(1 - y)]
+        return copy(S_C0, "CORE", 0, at, at, me, tp_c)
+
+    def to_core(i, c, block):
+        p, at = split(c)
+        part_of = abuf.at[source[i], block, p, :, at]
+        return copy(S_C, "CORE", i, part_of, part_of, me, tp_c)
+
+    rows_each = feat // n
 
     def pair(q):
-        return copy(S_PAIR, "PAIR", 0, ssend.at[1 - y, q], spair.at[q], me_y, tp)
+        at = pl.ds((q % 2) * (rows_each // 2), rows_each // 2)
+        src = ssend.at[1 - y, q // 2, at]
+        return copy(S_PAIR, "PAIR", 0, src, spair.at[q // 2, at], me_y, tp)
 
     def share(d):
         to = jnp.bitwise_xor(z, d)
@@ -272,15 +291,17 @@
         s, at, _ = piece(i)
         return copy(S_RC, "RC", i, part.at[s, 1 - core_of, :, at], crecv.at[s, :, at], me, tp_c)
 
-    def rx(i):
+    def rx(i, j=None):
         s, at, _ = piece(i)
-        return copy(S_RX, "RX", i, xsend.at[s, at], xrecv.at[s, at], me, tp_x)
+        if j is not None:
+            at = rows(y if j == 0 else 1 - y)
+        return copy(S_RX, "RX", i + (j or 0), xsend.at[s, at], xrecv.at[s, at], me, tp_x)
 
     def gc(i):
-        return copy(S_GC, "GC", i, gpart.at[i], gcore.at[i], me, tp_c)
+        return copy(S_GC, "GC", i, gpart.at[i, 0:1], gcore.at[i, 0:1], me, tp_c)
 
     def gxc(i):
-        return copy(S_GX, "GX", i, gtwo.at[i], gx.at[i], me, tp_x)
+        return copy(S_GX, "GX", i, gtwo.at[i, 0:1], gx.at[i, 0:1], me, tp_x)
 
     def back(i, j):
         s = source[i]
@@ -291,33 +312,35 @@
 
     def back_g(i, j):
         to = 2 * source[i] + (y if j == 0 else 1 - y)
-        return copy(S_RG, "RG", 0, gsend.at[i + 1], gret.at[me], to, tp)
-
-    def take(i, p, gate=None):
+        return copy(S_RG, "RG", 0, gsend.at[i + 1, 0:1], gret.at[me, 0:1], to, tp)
+
+    def take(i, c, gate=None):
         def run():
-            landed("ZF", 2 * source[i] + p, zbuf.at[source[i], p])
-
-            @pl.when(inner)
+            p, at = split(c)
+            landed("ZF", 4 * source[i] + c, zbuf.at[source[i], p, :, at])
+
+            @pl.when(low_inner if i == 1 else inner)
             def _():
-                z_relay(i, p).start()
+                z_relay(i, c).start()
 
         if gate is None:
             run()
         else:
             pl.when(gate)(run)
 
-    def spread(i, p):
-        moved = dot_f32(cperm[i], zbuf[source[i], p], ((1,), (0,))).astype(BF)
-        abuf[source[i], tp, p, rows(y)] = moved[0:cap]
-        ysend[i, p] = moved[cap:both_rows]
-        yf(i, p, tp).start()
-        fx(i, 0, p).start()
-
-    def crossed(i):
-        for p in range(2):
-            landed("YF", 2 * (i - 1) + p, abuf.at[source[i], tp, p, rows(1 - y)])
-            fx(i, 1, p).start()
-            to_core(i, p, tp).start()
+    def spread(i, c):
+        p, at = split(c)
+        moved = dot_f32(cperm[i], zbuf[source[i], p, :, at], ((1,), (0,))).astype(BF)
+        abuf[source[i], tp, p, rows(y), at] = moved[0:cap]
+        ysend[i, p, :, at] = moved[cap:both_rows]
+        yf(i, c).start()
+        fx(i, 0, c).start()
+
+    def crossed(i, c):
+        p, at = split(c)
+        landed("YF", 4 * (i - 1) + c, abuf.at[source[i], tp, p, rows(1 - y), at])
+        fx(i, 1, c).start()
+        to_core(i, c, tp).start()
 
     def ready(i):
         yw_in(i).wait_recv()
@@ -326,9 +349,10 @@
         else:
             landed("CORE", i, abuf.at[source[i], 0:2])
 
-    def joined(i, p):
-        landed("FX", 2 * (i - 1) + p, abuf.at[source[i], tp_x, p])
-        to_core(i, p, tp_x).start()
+    def joined(i, c):
+        p, at = split(c)
+        landed("FX", 4 * (i - 1) + c, abuf.at[source[i], tp_x, p, :, at])
+        to_core(i, c, tp_x).start()
 
     def compute(i):
         s, at, m = piece(i)
@@ -384,41 +408,47 @@
         gc(i).start()
 
     def core_sum(i):
-        s, at, _ = piece(i)
+        s, whole, _ = piece(i)
         rc(i).wait_recv()
-        xsend[s, at] = (
-            part[s, core_of, 1 - half_of, at].astype(F32) + crecv[s, 1 - half_of, at].astype(F32)
-        ).astype(BF)
-        rx(i).start()
+        for j in (0, 1) if i == planes else (None,):
+            at = whole if j is None else rows(y if j == 0 else 1 - y)
+            xsend[s, at] = (
+                part[s, core_of, 1 - half_of, at].astype(F32)
+                + crecv[s, 1 - half_of, at].astype(F32)
+            ).astype(BF)
+            rx(i, j).start()
         gc(i).wait_recv()
-        gtwo[i] = gpart[i] + gcore[i]
+        gtwo[i, 0:1] = gpart[i, 0:1] + gcore[i, 0:1]
         gxc(i).start()
-        keep[s, at] = part[s, core_of, half_of, at].astype(F32) + crecv[s, half_of, at].astype(F32)
+        keep[s, whole] = part[s, core_of, half_of, whole].astype(F32) + crecv[
+            s, half_of, whole
+        ].astype(F32)
 
     def give_back(i):
-        s, at, _ = piece(i)
-        rx(i).wait_recv()
-        total = (keep[s, at] + xrecv[s, at].astype(F32)).astype(BF)
+        s, whole, _ = piece(i)
+        if i == planes:
+            for j in range(2):
+                at = rows(y if j == 0 else 1 - y)
+                rx(i, j).wait_recv()
+                rsend[s, at] = (keep[s, at] + xrecv[s, at].astype(F32)).astype(BF)
+                back(i - 1, j).start()
+        else:
+            rx(i).wait_recv()
+            total = (keep[s, whole] + xrecv[s, whole].astype(F32)).astype(BF)
+            if i == 0:
+                ret[me] = total
+            else:
+                rsend[s, whole] = total
+                for j in (1,) if i == 1 else (0, 1):
+                    back(max(i - 1, 0), j).start()
+        gxc(i).wait_recv()
+        summed = gtwo[i, 0:1] + gx[i, 0:1]
         if i == 0:
-            ret[me] = total
+            gret[me, 0:1] = summed
         else:
-            rsend[s, at] = total
-            if i == 1:
-                back(0, 1).start()
-            else:
-                back(i - 1, 0).start()
-                back(i - 1, 1).start()
-        gxc(i).wait_recv()
-        summed = gtwo[i] + gx[i]
-        if i == 0:
-            gret[me] = summed
-        else:
-            gsend[i] = summed
-            if i == 1:
-                back_g(0, 1).start()
-            else:
-                back_g(i - 1, 0).start()
-                back_g(i - 1, 1).start()
+            gsend[i, 0:1] = summed
+            for j in (1,) if i == 1 else (0, 1):
+                back_g(i - 1, j).start()
 
     for load in loads[0:2]:
         load.wait()
@@ -441,23 +471,28 @@
         @pl.when(there)
         def _():
             zt_own(up).start()
-            z_own(up, 0).start()
-            z_own(up, 1).start()
+            for c in pieces_of:
+                z_own(up, c).start()
 
     read_tile(0)
+    loads[8].wait()
+    for j in range(n):
+        ssend[j % 2, j // 2] = dot_f32(
+            xg[1, :, j * rows_each : (j + 1) * rows_each], shv[...], ((0,), (0,))
+        ).astype(BF)
+    for q in range(planes):
+        pair(q).start()
     other = cperm[0, cap:both_rows, :]
     for p in range(2):
         ysend[0, p] = dot_f32(other, xg[p, :, columns(tp)], ((1,), (0,))).astype(BF)
-        yf(0, p, tp).start()
         ysend[planes, p] = dot_f32(other, xg[p, :, columns(tp_x)], ((1,), (0,))).astype(BF)
-        yf(0, p, tp_x).start()
     own = cperm[0, 0:cap, :]
     for b in range(4):
         for p in range(2):
             abuf[z, b, p, rows(y)] = dot_f32(
                 own, xg[p, :, b * quarter : (b + 1) * quarter], ((1,), (0,))
             ).astype(BF)
-    for load in loads[4:9]:
+    for load in loads[4:8]:
         load.wait()
     compute(0)
 
@@ -468,64 +503,68 @@
         def _():
             zt_relay(i).start()
 
+    late_second = jnp.logical_not(low_inner)
+    late_third = jnp.logical_not(high_inner)
     tile_in(1)
-    pl.when(inner)(functools.partial(tile_in, 2))
+    pl.when(low_inner)(functools.partial(tile_in, 2))
+    pl.when(high_inner)(functools.partial(tile_in, 3))
     read_tile(1)
     ohid_ref[...] = dot_f32(xg[1], sdv[...], ((1,), (0,))).astype(BF)
-    rows_each = feat // n
-    for j in range(n):
-        ssend[j % 2, j // 2] = dot_f32(
-            xg[1, :, j * rows_each : (j + 1) * rows_each], shv[...], ((0,), (0,))
-        ).astype(BF)
-
-    take(1, 0)
-    take(2, 0, inner)
-    spread(1, 0)
     core_sum(0)
-    pair(0).start()
-    take(1, 1)
-    take(2, 1, inner)
-    spread(1, 1)
-    pair(1).start()
-    landed("Y0", 0, abuf.at[z, 0:2, :, rows(1 - y)])
-    for p in range(2):
-        to_core(0, p, tp).start()
-        to_core(0, p, tp_x).start()
-    pl.when(inner)(functools.partial(tile_in, 3))
-    crossed(1)
-    ready(0)
-    compute(1)
-    pl.when(outer)(functools.partial(tile_in, 2))
-    take(2, 0, outer)
+    for c in pieces_of:
+        take(1, c)
+        take(2, c, low_inner)
+        take(3, c, high_inner)
+        spread(1, c)
+    for q in range(planes, 2 * planes):
+        pair(q).start()
+    pl.when(late_second)(functools.partial(tile_in, 2))
+    crossed(1, 0)
     read_tile(2)
-    take(3, 0, inner)
-    spread(2, 0)
-    pair(2).start()
+    for c in pieces_of:
+        take(2, c, late_second)
+        spread(2, c)
+        if c < 3:
+            crossed(1, c + 1)
+
+    @pl.when(high_inner)
+    def _():
+        for c in pieces_of:
+            z_relay(1, c).start()
+
+    pl.when(late_third)(functools.partial(tile_in, 3))
+    read_tile(3)
     joined(1, 0)
-    core_sum(1)
-    take(2, 1, outer)
-    take(3, 1, inner)
-    spread(2, 1)
-    pair(3).start()
     joined(1, 1)
-    crossed(2)
-
+    for c in pieces_of:
+        crossed(2, c)
+        take(3, c, late_third)
+        spread(3, c)
+        if c < 2:
+            joined(1, c + 2)
+    for c in pieces_of:
+        y_own(c, tp).start()
+        y_own(c, tp_x).start()
     ready(1)
     compute(2)
-    give_back(0)
-    pl.when(outer)(functools.partial(tile_in, 3))
-    take(3, 0, outer)
-    read_tile(3)
-    spread(3, 0)
+    joined(2, 0)
+    joined(2, 1)
+    crossed(3, 0)
+    joined(2, 2)
+    crossed(3, 1)
+    joined(2, 3)
+    crossed(3, 2)
+    crossed(3, 3)
     core_sum(2)
-    joined(2, 0)
-    take(3, 1, outer)
-    spread(3, 1)
-    joined(2, 1)
-    give_back(1)
-    crossed(3)
+    landed("PAIR", 0, spair)
+    for q in range(planes):
+        ssum[q] = (ssend[y, q].astype(F32) + spair[q].astype(F32)).astype(BF)
+    srecv[z] = ssum[z]
+    for d in range(1, planes):
+        share(d).start()
     ready(2)
     compute(3)
+    give_back(0)
 
     names = lax.broadcasted_iota(jnp.int32, (128, tok_rows), 0)
     named_t = jnp.zeros((128, tok_rows), F32)
@@ -535,41 +574,35 @@
     for e in range(n):
         perm[e] = jnp.where(slot == rank_t[e : e + 1, :], named_t[e : e + 1, :], 0.0).astype(BF)
 
-    give_back(2)
     core_sum(3)
-    landed("PAIR", 0, spair)
-    for q in range(planes):
-        ssum[q] = (ssend[y, q].astype(F32) + spair[q].astype(F32)).astype(BF)
-    srecv[z] = ssum[z]
-    for d in range(1, planes):
-        share(d).start()
-    joined(3, 0)
-    joined(3, 1)
+    for c in pieces_of:
+        joined(3, c)
     ready(3)
     compute(4)
+    give_back(2)
+    core_sum(4)
+    landed("Y0", 0, abuf.at[z, 0:2, :, rows(1 - y)])
+    for p in range(2):
+        own_to_core(p, tp).start()
+        own_to_core(p, tp_x).start()
     give_back(3)
-    core_sum(4)
+    ready(0)
+    compute(1)
+    core_sum(1)
 
     d_all = dgu[...].reshape(n * cap, 2 * units)
     h_all = hw[...].reshape(n * cap, units)
     for b in range(4):
         at = slice(b * quarter, (b + 1) * quarter)
         grad = dot_f32(abuf[:, b, 0].reshape(n * cap, quarter), d_all, ((0,), (0,))).astype(BF)
-        gradv[0, at, :] = grad[:, 0:units]
-        gradv[1, at, :] = grad[:, units : 2 * units]
-        wdv[:, at] = dot_f32(
+        og_ref[at, :] = grad[:, 0:units]
+        ou_ref[at, :] = grad[:, units : 2 * units]
+        od_ref[:, at] = dot_f32(
             h_all, abuf[:, b, 1].reshape(n * cap, quarter), ((0,), (0,))
         ).astype(BF)
 
-    stores = [
-        pltpu.make_async_copy(gradv.at[0], og_ref, store_sem.at[0]),
-        pltpu.make_async_copy(gradv.at[1], ou_ref, store_sem.at[1]),
-        pltpu.make_async_copy(wdv, od_ref, store_sem.at[2]),
-    ]
-    for store in stores:
-        store.start()
-
     give_back(4)
+    give_back(1)
 
     landed("SHARE", 0, srecv.at[0 : planes - 1])
     sums = srecv[0].astype(F32)
@@ -577,10 +610,10 @@
         sums = sums + srecv[j].astype(F32)
     osh_ref[...] = sums
 
-    landed("RG", 0, gret.at[0 : n - 1])
+    landed("RG", 0, gret.at[0, 0 : n - 1])
     pieces = []
     for e in range(n):
-        full = gret[e]
+        full = jnp.broadcast_to(gret[e, 0:1], (8, both_rows))
         row = jnp.where(at_zero, full[:, 0:cap], full[:, cap:both_rows]).astype(BF)
         pieces.append(dot_f32(row, perm[e], ((1,), (0,)))[0:1, :])
     pieces.append(jnp.zeros((128 - n, tok_rows), F32))
@@ -594,9 +627,6 @@
         perm[...].reshape(n * cap, tok_rows), ret[...].reshape(n * cap, quarter), ((0,), (0,))
     ).astype(BF)
 
-    for store in stores:
-        store.wait()
-
     @pl.when(inner)
     def _():
         left(S_ZO, zbuf.at[0:2])
@@ -616,24 +646,20 @@
     left(S_C, abuf.at[0 : planes - 1, 0:2])
     left(S_RC, crecv)
     left(S_RX, xsend)
-    left(S_GC, gpart)
-    left(S_GX, gtwo)
+    left(S_GC, gpart.at[0, 0 : planes + 1])
+    left(S_GX, gtwo.at[0, 0 : planes + 1])
     left(S_RE, ret.at[0 : n - 1])
-    left(S_RG, gret.at[0 : n - 1])
+    left(S_RG, gret.at[0, 0 : n - 1])
     left(S_SHARE, srecv.at[0 : planes - 1])
     left(S_PAIR, spair)
 
 
 def pass_on(*refs):
-    count = (len(refs) - 2) // 3
-    ins, outs, held = refs[:count], refs[count : 2 * count], refs[2 * count : 3 * count]
-    in_sem, out_sem = refs[-2:]
-    loads = [pltpu.make_async_copy(ins[i], held[i], in_sem.at[i]) for i in range(count)]
-    stores = [pltpu.make_async_copy(held[i], outs[i], out_sem.at[i]) for i in range(count)]
-    for load in loads:
-        load.start()
-    for load, store in zip(loads, stores):
-        load.wait()
+    count = len(refs) // 2
+    stores = [
+        pltpu.make_async_copy(refs[i], refs[count + i], refs[-1].at[i]) for i in range(count)
+    ]
+    for store in stores:
         store.start()
     for store in stores:
         store.wait()
@@ -641,15 +667,13 @@
 
 def hand_over(arrays):
     count = len(arrays)
-    hbm = pl.BlockSpec(memory_space=pl.ANY)
     return pl.pallas_call(
         pass_on,
         out_shape=tuple(jax.ShapeDtypeStruct(a.shape, a.dtype) for a in arrays),
-        in_specs=[hbm] * count,
-        out_specs=tuple([hbm] * count),
-        scratch_shapes=[pltpu.VMEM(a.shape, a.dtype) for a in arrays]
-        + [pltpu.SemaphoreType.DMA((count,))] * 2,
-    )(*arrays)
+        in_specs=[pl.BlockSpec(memory_space=pltpu.VMEM)] * count,
+        out_specs=tuple([pl.BlockSpec(memory_space=pl.ANY)] * count),
+        scratch_shapes=[pltpu.SemaphoreType.DMA((count,))],
+    )(*(pltpu.with_memory_space_constraint(a, pltpu.VMEM) for a in arrays))
 
 
 def fused_shards(
@@ -672,13 +696,13 @@
     quarter = feat // 4
     planes = n // 2
     out_shape = (
-        jax.ShapeDtypeStruct((tok_rows, quarter), BF),
-        jax.ShapeDtypeStruct((top, tok_rows), F32),
-        jax.ShapeDtypeStruct((feat, units), BF),
-        jax.ShapeDtypeStruct((feat, units), BF),
-        jax.ShapeDtypeStruct((units, feat), BF),
-        jax.ShapeDtypeStruct((tok_rows, hid), BF),
-        jax.ShapeDtypeStruct((feat // n, hid), F32),
+        pltpu.VMEM((tok_rows, quarter), BF),
+        pltpu.VMEM((top, tok_rows), F32),
+        pltpu.VMEM((feat, units), BF),
+        pltpu.VMEM((feat, units), BF),
+        pltpu.VMEM((units, feat), BF),
+        pltpu.VMEM((tok_rows, hid), BF),
+        pltpu.VMEM((feat // n, hid), F32),
     )
     vmem = pl.BlockSpec(memory_space=pltpu.VMEM)
     hbm = pl.BlockSpec(memory_space=pl.ANY)
@@ -687,7 +711,7 @@
         functools.partial(kernel, n, cap),
         out_shape=out_shape,
         in_specs=[hbm] * 9,
-        out_specs=(vmem, vmem, hbm, hbm, hbm, vmem, vmem),
+        out_specs=(vmem,) * 7,
         scratch_shapes=[
             pltpu.VMEM((2, tok_rows, feat), BF),
             pltpu.VMEM((top, tok_rows), F32),
@@ -704,7 +728,6 @@
             pltpu.VMEM((feat, 2 * units), BF),
             pltpu.VMEM((units, feat), BF),
             pltpu.VMEM((feat, hid), BF),
-            pltpu.VMEM((2, feat, units), BF),
             pltpu.VMEM((planes, 2 * cap, units), BF),
             pltpu.VMEM((planes, 2 * cap, 2 * units), BF),
             pltpu.VMEM((planes, 2, 2, 2 * cap, quarter), BF),
@@ -727,21 +750,25 @@
             pltpu.SemaphoreType.DMA((SENDS,)),
             pltpu.SemaphoreType.DMA((ARRIVALS,)),
             pltpu.SemaphoreType.DMA((9,)),
-            pltpu.SemaphoreType.DMA((3,)),
         ],
         compiler_params=pltpu.CompilerParams(
-            collective_id=0, has_side_effects=True, vmem_limit_bytes=60 * 1024 * 1024
+            collective_id=0, has_side_effects=True, vmem_limit_bytes=48 * 1024 * 1024
         ),
     )(
-        tokens,
-        cotangent,
-        route_weights.T,
-        routes.T,
-        gate_proj[0],
-        up_proj[0],
-        down_proj[0],
-        shared_down,
-        shared_hidden,
+        *(
+            pltpu.with_memory_space_constraint(a, pltpu.HBM)
+            for a in (
+                tokens,
+                cotangent,
+                route_weights.T,
+                routes.T,
+                gate_proj[0],
+                up_proj[0],
+                down_proj[0],
+                shared_down,
+                shared_hidden,
+            )
+        )
     )
     outs = hand_over(outs)
     return outs[0], outs[1].T, outs[2][None], outs[3][None], outs[4][None], outs[5], outs[6]

time: 58.5 us -> 51.1 us (0.87)
  Pallas kernels: 57.7 us -> 49.8 us
    pallas_call x1, Pallas kernels: 55.3 us -> 48.5 us  [fused_shards(): pl.pallas_call(functools.partial(kernel, n, cap), out_shape=out_shape, in...]
    pallas_call x1, Pallas kernels: 2.43 us -> 1.3 us  [hand_over(): pl.pallas_call(pass_on, out_shape=tuple((jax.ShapeDtypeStruct(a.shape, a....]
where the time goes in v2:
time: 51.1 us; the launch traced here: 50.4 us
  Pallas kernels  49.8 us (97%)
  between operations  0.64 us (1%)
    pallas_call x1, Pallas kernels, fused_shards(): pl.pallas_call(functools.partial(kernel, n, cap), out_shape=out_shape, in...  48.5 us
    pallas_call x1, Pallas kernels, hand_over(): pl.pallas_call(pass_on, out_shape=tuple((jax.ShapeDtypeStruct(a.shape, a....  1.3 us

profile of v2, /device:TPU:0, one launch (start us, length us, event | category | flops | bytes accessed | tf_op | source)
XLA Modules:
  0.0 50.4 jit_solution(16795295326004214164)
XLA Ops:
  0.6 48.5 %shard_map.144 = (bf16[128,512]{1,0:T(8,128)(2,1)S(1)}, f32[2,128]{1,0:T(2,128)S(1)}, bf16[2048,128]{1,0:T(8,128)(2,1)S(1)}, bf16[2048,128]{1,0:T(8,128)(2,1)S(1...) custom-call(bf16[128,2048]{1,0:T(8,128)(2,1)} %tok_ref.1, ...), custom_call_target="tpu_custom_call" | custom-call | tf_op jit(solution)/shard_map/pallas_call | solution.py:710
  49.1 1.3 %shard_map.145 = (bf16[128,512]{1,0:T(8,128)(2,1)}, f32[2,128]{1,0:T(2,128)}, bf16[2048,128]{1,0:T(8,128)(2,1)}, bf16[2048,128]{1,0:T(8,128)(2,1)}, bf16[128,204...) custom-call(bf16[128,512]{1,0:T(8,128)(2,1)S(1)} %get-tuple-element.21.refs_0_, ...), custom_call_target="tpu_custom_call" | custom-call | tf_op jit(solution)/shard_map/pallas_call | solution.py:670

commit v3 on v2

--- a/solution.py
+++ b/solution.py
@@ -20,8 +20,8 @@
     "YW": 4,
     "FX": 12,
     "CORE": 4,
-    "RC": 5,
-    "RX": 6,
+    "RC": 10,
+    "RX": 7,
     "GC": 5,
     "GX": 5,
     "RE": 1,
@@ -173,7 +173,7 @@
             )
         )
     ]
-    for load in loads:
+    for load in loads[0:4]:
         load.start()
 
     before = jnp.where(
@@ -287,15 +287,19 @@
             return z, rows(1 - y), cap
         return source[i - 1], pl.ds(0, both_rows), both_rows
 
-    def rc(i):
+    def rc(i, kept):
         s, at, _ = piece(i)
-        return copy(S_RC, "RC", i, part.at[s, 1 - core_of, :, at], crecv.at[s, :, at], me, tp_c)
-
-    def rx(i, j=None):
-        s, at, _ = piece(i)
-        if j is not None:
-            at = rows(y if j == 0 else 1 - y)
-        return copy(S_RX, "RX", i + (j or 0), xsend.at[s, at], xrecv.at[s, at], me, tp_x)
+        h = half_of if kept else 1 - half_of
+        src = part.at[s, 1 - core_of, h, at]
+        return copy(S_RC, "RC", 2 * i + kept, src, crecv.at[s, h, at], me, tp_c)
+
+    def halves(i):
+        return ((0, rows(0)), (1, rows(1))) if i >= planes - 1 else ((0, piece(i)[1]),)
+
+    def rx(i, j, at):
+        s = piece(i)[0]
+        at_sem = i + j + (1 if i == planes else 0)
+        return copy(S_RX, "RX", at_sem, xsend.at[s, at], xrecv.at[s, at], me, tp_x)
 
     def gc(i):
         return copy(S_GC, "GC", i, gpart.at[i, 0:1], gcore.at[i, 0:1], me, tp_c)
@@ -303,15 +307,13 @@
     def gxc(i):
         return copy(S_GX, "GX", i, gtwo.at[i, 0:1], gx.at[i, 0:1], me, tp_x)
 
-    def back(i, j):
+    def back(i, block_y):
         s = source[i]
-        block_y = y if j == 0 else 1 - y
-        return copy(
-            S_RE, "RE", 0, rsend.at[s, rows(block_y)], ret.at[me], 2 * s + block_y, tp
-        )
-
-    def back_g(i, j):
-        to = 2 * source[i] + (y if j == 0 else 1 - y)
+        src = rsend.at[s, rows(block_y)]
+        return copy(S_RE, "RE", 0, src, ret.at[me], 2 * s + block_y, tp)
+
+    def back_g(i, block_y):
+        to = 2 * source[i] + block_y
         return copy(S_RG, "RG", 0, gsend.at[i + 1, 0:1], gret.at[me, 0:1], to, tp)
 
     def take(i, c, gate=None):
@@ -319,7 +321,7 @@
             p, at = split(c)
             landed("ZF", 4 * source[i] + c, zbuf.at[source[i], p, :, at])
 
-            @pl.when(low_inner if i == 1 else inner)
+            @pl.when(low_inner if i == 1 and c > 1 else inner)
             def _():
                 z_relay(i, c).start()
 
@@ -391,7 +393,8 @@
         for b in range(4):
             cols = slice(b * quarter, (b + 1) * quarter)
             part[s, b % 2, b // 2, at] = dot_f32(d_both, wgu[cols, :], ((1,), (1,))).astype(BF)
-        rc(i).start()
+        rc(i, 0).start()
+        rc(i, 1).start()
         sums = lax.dot_general(
             jnp.ones((8, units), F32),
             hidden * backed,
@@ -409,46 +412,50 @@
 
     def core_sum(i):
         s, whole, _ = piece(i)
-        rc(i).wait_recv()
-        for j in (0, 1) if i == planes else (None,):
-            at = whole if j is None else rows(y if j == 0 else 1 - y)
+        rc(i, 0).wait_recv()
+        for j, at in halves(i):
             xsend[s, at] = (
                 part[s, core_of, 1 - half_of, at].astype(F32)
                 + crecv[s, 1 - half_of, at].astype(F32)
             ).astype(BF)
-            rx(i, j).start()
-        gc(i).wait_recv()
-        gtwo[i, 0:1] = gpart[i, 0:1] + gcore[i, 0:1]
-        gxc(i).start()
+            rx(i, j, at).start()
+            if j == 0:
+                gc(i).wait_recv()
+                gtwo[i, 0:1] = gpart[i, 0:1] + gcore[i, 0:1]
+                gxc(i).start()
+        rc(i, 1).wait_recv()
         keep[s, whole] = part[s, core_of, half_of, whole].astype(F32) + crecv[
             s, half_of, whole
         ].astype(F32)
 
     def give_back(i):
         s, whole, _ = piece(i)
-        if i == planes:
-            for j in range(2):
-                at = rows(y if j == 0 else 1 - y)
-                rx(i, j).wait_recv()
-                rsend[s, at] = (keep[s, at] + xrecv[s, at].astype(F32)).astype(BF)
-                back(i - 1, j).start()
-        else:
-            rx(i).wait_recv()
-            total = (keep[s, whole] + xrecv[s, whole].astype(F32)).astype(BF)
+        for j, at in halves(i):
+            rx(i, j, at).wait_recv()
+            total = (keep[s, at] + xrecv[s, at].astype(F32)).astype(BF)
             if i == 0:
                 ret[me] = total
             else:
-                rsend[s, whole] = total
-                for j in (1,) if i == 1 else (0, 1):
-                    back(max(i - 1, 0), j).start()
-        gxc(i).wait_recv()
-        summed = gtwo[i, 0:1] + gx[i, 0:1]
-        if i == 0:
-            gret[me, 0:1] = summed
-        else:
-            gsend[i, 0:1] = summed
-            for j in (1,) if i == 1 else (0, 1):
-                back_g(i - 1, j).start()
+                rsend[s, at] = total
+            if i == 1:
+                back(0, 1 - y).start()
+            if i == 2:
+                back(1, 0).start()
+                back(1, 1).start()
+            if i > 2:
+                back(i - 1, j).start()
+            if j == 0:
+                gxc(i).wait_recv()
+                summed = gtwo[i, 0:1] + gx[i, 0:1]
+                if i == 0:
+                    gret[me, 0:1] = summed
+                else:
+                    gsend[i, 0:1] = summed
+                if i == 1:
+                    back_g(0, 1 - y).start()
+                if i > 1:
+                    back_g(i - 1, 0).start()
+                    back_g(i - 1, 1).start()
 
     for load in loads[0:2]:
         load.wait()
@@ -462,6 +469,8 @@
     )
     for load in loads[2:4]:
         load.wait()
+    for load in loads[4:9]:
+        load.start()
     pl.semaphore_wait(
         barrier, 3 + jnp.where(z > 0, 1, 0) + jnp.where(z < planes - 1, 1, 0)
     )
@@ -504,7 +513,6 @@
             zt_relay(i).start()
 
     late_second = jnp.logical_not(low_inner)
-    late_third = jnp.logical_not(high_inner)
     tile_in(1)
     pl.when(low_inner)(functools.partial(tile_in, 2))
     pl.when(high_inner)(functools.partial(tile_in, 3))
@@ -521,27 +529,52 @@
     pl.when(late_second)(functools.partial(tile_in, 2))
     crossed(1, 0)
     read_tile(2)
+
+    @pl.when(outer)
+    def _():
+        for c in pieces_of[1:]:
+            crossed(1, c)
+
     for c in pieces_of:
         take(2, c, late_second)
         spread(2, c)
         if c < 3:
-            crossed(1, c + 1)
+            pl.when(inner)(functools.partial(crossed, 1, c + 1))
 
     @pl.when(high_inner)
     def _():
-        for c in pieces_of:
+        for c in pieces_of[2:]:
             z_relay(1, c).start()
 
-    pl.when(late_third)(functools.partial(tile_in, 3))
-    read_tile(3)
+    @pl.when(low_inner)
+    def _():
+        tile_in(3)
+        take(3, 0)
+
     joined(1, 0)
+    take(3, 1, low_inner)
     joined(1, 1)
-    for c in pieces_of:
-        crossed(2, c)
-        take(3, c, late_third)
+    take(3, 2, low_inner)
+    crossed(2, 0)
+    joined(1, 2)
+    take(3, 3, low_inner)
+    joined(1, 3)
+    crossed(2, 1)
+
+    def open_third():
+        pl.when(outer)(functools.partial(tile_in, 3))
+        read_tile(3)
+        for c in pieces_of[0:2]:
+            take(3, c, outer)
+            spread(3, c)
+
+    pl.when(z > 0)(open_third)
+    crossed(2, 2)
+    crossed(2, 3)
+    pl.when(z == 0)(open_third)
+    for c in pieces_of[2:]:
+        take(3, c, outer)
         spread(3, c)
-        if c < 2:
-            joined(1, c + 2)
     for c in pieces_of:
         y_own(c, tp).start()
         y_own(c, tp_x).start()

time: 51.1 us -> 49.2 us (0.963)
  the two profiles are of different devices: /device:TPU:0 before, /device:TPU:24 now
where the time goes in v3:
time: 49.2 us; the launch traced here: 49.1 us
  Pallas kernels  48.4 us (98%)
  between operations  0.64 us (1%)
    pallas_call x1, Pallas kernels, fused_shards(): pl.pallas_call(functools.partial(kernel, n, cap), out_shape=out_shape, in...  47.1 us
    pallas_call x1, Pallas kernels, hand_over(): pl.pallas_call(pass_on, out_shape=tuple((jax.ShapeDtypeStruct(a.shape, a....  1.3 us

profile of v3, /device:TPU:24, one launch (start us, length us, event | category | flops | bytes accessed | tf_op | source)
XLA Modules:
  0.0 49.1 jit_solution(3901812410998257075)
XLA Ops:
  0.6 47.1 %shard_map.144 = (bf16[128,512]{1,0:T(8,128)(2,1)S(1)}, f32[2,128]{1,0:T(2,128)S(1)}, bf16[2048,128]{1,0:T(8,128)(2,1)S(1)}, bf16[2048,128]{1,0:T(8,128)(2,1)S(1...) custom-call(bf16[128,2048]{1,0:T(8,128)(2,1)} %tok_ref.1, ...), custom_call_target="tpu_custom_call" | custom-call | tf_op jit(solution)/shard_map/pallas_call | solution.py:743
  47.8 1.3 %shard_map.145 = (bf16[128,512]{1,0:T(8,128)(2,1)}, f32[2,128]{1,0:T(2,128)}, bf16[2048,128]{1,0:T(8,128)(2,1)}, bf16[2048,128]{1,0:T(8,128)(2,1)}, bf16[128,204...) custom-call(bf16[128,512]{1,0:T(8,128)(2,1)S(1)} %get-tuple-element.21.refs_0_, ...), custom_call_target="tpu_custom_call" | custom-call | tf_op jit(solution)/shard_map/pallas_call | solution.py:703

commit v4 on v3

--- a/solution.py
+++ b/solution.py
@@ -115,8 +115,9 @@
     low_inner = z == 1
     high_inner = z == planes - 2
     first = jnp.where(z == 0, 1, z - 1)
-    second = jnp.where(z == 0, 2, jnp.where(low_inner, z + 1, 0))
-    source = [z, first, second, jnp.where(z == planes - 1, 1, planes - 1)]
+    second = jnp.where(z == 0, 2, jnp.where(low_inner, planes - 1, 0))
+    third = jnp.where(z == planes - 1, 1, jnp.where(low_inner, 2, planes - 1))
+    source = [z, first, second, third]
     pieces_of = range(4)
     part_cols = quarter // 2
 
@@ -512,21 +513,18 @@
         def _():
             zt_relay(i).start()
 
-    late_second = jnp.logical_not(low_inner)
     tile_in(1)
-    pl.when(low_inner)(functools.partial(tile_in, 2))
-    pl.when(high_inner)(functools.partial(tile_in, 3))
+    pl.when(inner)(functools.partial(tile_in, 3))
     read_tile(1)
     ohid_ref[...] = dot_f32(xg[1], sdv[...], ((1,), (0,))).astype(BF)
     core_sum(0)
     for c in pieces_of:
         take(1, c)
-        take(2, c, low_inner)
-        take(3, c, high_inner)
+        take(3, c, inner)
         spread(1, c)
     for q in range(planes, 2 * planes):
         pair(q).start()
-    pl.when(late_second)(functools.partial(tile_in, 2))
+    tile_in(2)
     crossed(1, 0)
     read_tile(2)
 
@@ -536,7 +534,7 @@
             crossed(1, c)
 
     for c in pieces_of:
-        take(2, c, late_second)
+        take(2, c)
         spread(2, c)
         if c < 3:
             pl.when(inner)(functools.partial(crossed, 1, c + 1))
@@ -546,18 +544,10 @@
         for c in pieces_of[2:]:
             z_relay(1, c).start()
 
-    @pl.when(low_inner)
-    def _():
-        tile_in(3)
-        take(3, 0)
-
     joined(1, 0)
-    take(3, 1, low_inner)
     joined(1, 1)
-    take(3, 2, low_inner)
     crossed(2, 0)
     joined(1, 2)
-    take(3, 3, low_inner)
     joined(1, 3)
     crossed(2, 1)
 

time: 49.2 us -> 49.1 us (level)
  the two profiles are of different devices: /device:TPU:24 before, /device:TPU:0 now
where the time goes in v4:
time: 49.1 us; the launch traced here: 48.2 us
  Pallas kernels  47.5 us (97%)
  between operations  0.64 us (1%)
    pallas_call x1, Pallas kernels, fused_shards(): pl.pallas_call(functools.partial(kernel, n, cap), out_shape=out_shape, in...  46.2 us
    pallas_call x1, Pallas kernels, hand_over(): pl.pallas_call(pass_on, out_shape=tuple((jax.ShapeDtypeStruct(a.shape, a....  1.3 us

profile of v4, /device:TPU:0, one launch (start us, length us, event | category | flops | bytes accessed | tf_op | source)
XLA Modules:
  0.0 48.2 jit_solution(9665156677511996244)
XLA Ops:
  0.6 46.2 %shard_map.144 = (bf16[128,512]{1,0:T(8,128)(2,1)S(1)}, f32[2,128]{1,0:T(2,128)S(1)}, bf16[2048,128]{1,0:T(8,128)(2,1)S(1)}, bf16[2048,128]{1,0:T(8,128)(2,1)S(1...) custom-call(bf16[128,2048]{1,0:T(8,128)(2,1)} %tok_ref.1, ...), custom_call_target="tpu_custom_call" | custom-call | tf_op jit(solution)/shard_map/pallas_call | solution.py:733
  46.9 1.3 %shard_map.145 = (bf16[128,512]{1,0:T(8,128)(2,1)}, f32[2,128]{1,0:T(2,128)}, bf16[2048,128]{1,0:T(8,128)(2,1)}, bf16[2048,128]{1,0:T(8,128)(2,1)}, bf16[128,204...) custom-call(bf16[128,512]{1,0:T(8,128)(2,1)S(1)} %get-tuple-element.21.refs_0_, ...), custom_call_target="tpu_custom_call" | custom-call | tf_op jit(solution)/shard_map/pallas_call | solution.py:693
